TPU v7x, 32 devices: a whole 2x2x4 slice. The times are simulated.
32 devices in a mesh: ep: 8 (over z, core), tp: 4 (over y, x).
Axes of the slice: x: 2, y: 2, z: 4, core: 2. Of those that a mesh axis runs over, the one named last changes fastest.
Arguments:
- query_rows: bfloat16 [6144, 1024], P('ep', 'tp'), may hold values from -600 to 600
- key_rows: bfloat16 [6144, 1024], P('ep', 'tp'), may hold values from -6 to 6
- value_rows: bfloat16 [6144, 1024], P('ep', 'tp'), may hold values from -6 to 6
- cum_gate: float32 [16, 6144], P('tp'), may hold values from -615 to 0, as said below
- out_weight: bfloat16 [1024, 2048], P(None, 'tp'), may hold values from -0.1875 to 0.1875
- moe_input: bfloat16 [1536, 2048], P('ep'), may hold values from -6 to 6
- moe_gain: float32 [2048], replicated, may hold values from 0.1 to 1.9
- routes: int32 [1536, 3], P('ep'), may hold values from 0 to 31, all different within a row; in each aligned block of 192 rows (0 to 191, 192 to 383, ...) at most 36 rows name the same one
- route_weight: float32 [1536, 3], P('ep'), may hold values from 0.2 to 1.5
- expert_gate: bfloat16 [32, 2048, 512], P('ep', None, 'tp'), may hold values from -0.125 to 0.125
- expert_up: bfloat16 [32, 2048, 512], P('ep', None, 'tp'), may hold values from -0.125 to 0.125
- expert_down: bfloat16 [32, 512, 2048], P('ep', None, 'tp'), may hold values from -0.25 to 0.25
- shared_gate: bfloat16 [2048, 512], P(None, 'tp'), may hold values from -0.125 to 0.125
- shared_up: bfloat16 [2048, 512], P(None, 'tp'), may hold values from -0.125 to 0.125
- shared_down: bfloat16 [512, 2048], P(None, 'tp'), may hold values from -0.25 to 0.25
Outputs:
- mixer_out: bfloat16 [6144, 2048], P('ep', 'tp')
- moe_out: bfloat16 [1536, 2048], P('ep', 'tp')
Inputs may be any that keep to these rules, and one draw needn't show every extreme that they name: Non-increasing along positions: cum_gate[h, t] is the sum of the log forget gates of head h over positions 0 to t. `routes`: the 3 experts of a token differ. In each aligned block of 192 tokens no expert is named by more than 36 tokens, a bound that some block reaches.
All inputs are finite; a program needn't handle non-finite values.
Results may differ from a plain program's by a relative error of at most 0.0068.
Values may be sent and summed in bfloat16 or wider, within the bound.
A program may use at most 64 MiB of HBM per device.

v0:
```python
import functools

import jax
import jax.numpy as jnp
from jax import lax
from jax.experimental import pallas as pl
from jax.experimental.pallas import tpu as pltpu
from jax.sharding import PartitionSpec as P

HEAD = 64
LANES = 128
CORES = 2

neg_fill = -1e30
norm_eps = 1e-06


def attention_kernel(
    heads,
    q_ref,
    kv_ref,
    gate_ref,
    normed_ref,
    rank_ref,
    out_ref,
    tokens,
    picks,
    held,
    acc,
    row_max,
    up_send,
    side_send,
    recv_sem,
    chip_send,
    plane_send,
    piece_recv,
    block_send,
    block_recv,
    own_sem,
    rank_send,
    rank_recv,
):
    rows = kv_ref.shape[0]
    width = kv_ref.shape[1] // 2
    pairs = width // LANES
    tile = 256 if rows % 256 == 0 else rows
    tiles = rows // tile
    me = lax.axis_index("ep")
    chips = lax.axis_size("ep") // CORES
    chip = me // CORES
    core = me % CORES
    other = 1 - core

    barrier = pltpu.get_barrier_semaphore()

    def loop(count, body):
        def step(index, carry):
            body(index)
            return carry

        lax.fori_loop(0, count, step, 0)

    def greet(**where):
        pl.semaphore_signal(barrier, inc=1, device_id=where)

    tp_count = lax.axis_size("tp")
    tp_me = lax.axis_index("tp")
    columns = normed_ref.shape[1] // tp_count

    def chip_at(turn):
        return lax.rem(chip + turn + 1, chips)

    def tp_at(turn):
        return lax.rem(tp_me + turn + 1, tp_count)

    ep_count = chips * CORES

    def ep_at(turn):
        return lax.rem(me + turn + 1, ep_count)

    loop(ep_count - 1, lambda turn: greet(ep=ep_at(turn)))
    loop(tp_count - 1, lambda turn: greet(tp=tp_at(turn)))
    pl.semaphore_wait(barrier, ep_count + tp_count - 2)

    def rank_copy(target, owner):
        return pltpu.make_async_remote_copy(
            src_ref=rank_ref.at[target],
            dst_ref=picks.at[owner],
            send_sem=rank_send.at[target],
            recv_sem=rank_recv.at[owner],
            device_id={"ep": target},
        )

    def up_copy(src, slot):
        return pltpu.make_async_remote_copy(
            src_ref=src,
            dst_ref=held.at[slot],
            send_sem=up_send.at[slot],
            recv_sem=recv_sem.at[slot],
            device_id={"ep": me + CORES},
        )

    def far_copy(target):
        return pltpu.make_async_remote_copy(
            src_ref=kv_ref,
            dst_ref=held.at[me],
            send_sem=up_send.at[target * CORES + core],
            recv_sem=recv_sem.at[me],
            device_id={"ep": target * CORES + core},
        )

    def side_copy(src, slot):
        return pltpu.make_async_remote_copy(
            src_ref=src,
            dst_ref=held.at[slot],
            send_sem=side_send.at[slot],
            recv_sem=recv_sem.at[slot],
            device_id={"ep": chip * CORES + other},
        )

    def lanes_of(index):
        return pl.ds(pl.multiple_of(index * columns, columns), columns)

    def chip_copy(target):
        return pltpu.make_async_remote_copy(
            src_ref=normed_ref.at[:, lanes_of(tp_me)],
            dst_ref=tokens.at[me, :, lanes_of(tp_me)],
            send_sem=chip_send.at[target],
            recv_sem=piece_recv.at[me, tp_me],
            device_id={"ep": target * CORES + core},
        )

    def plane_copy(slot, piece, target):
        place = tokens.at[slot, :, lanes_of(piece)]
        return pltpu.make_async_remote_copy(
            src_ref=place,
            dst_ref=place,
            send_sem=plane_send.at[slot, target],
            recv_sem=piece_recv.at[slot, piece],
            device_id={"tp": target},
        )

    def block_copy(src, slot):
        return pltpu.make_async_remote_copy(
            src_ref=src,
            dst_ref=tokens.at[slot],
            send_sem=block_send.at[slot],
            recv_sem=block_recv.at[slot],
            device_id={"ep": chip * CORES + other},
        )

    loop(chips - 1, lambda turn: chip_copy(chip_at(turn)).start())

    @pl.when(chip < chips - 1)
    def _():
        up_copy(kv_ref, me).start()

    reach = chips // 2
    far_count = jnp.maximum(chips - 1 - reach - chip, 0)
    loop(far_count, lambda turn: far_copy(chips - 1 - turn).start())

    @pl.when(core == 0)
    def _():
        side_copy(kv_ref, me).start()

    block_copy(normed_ref, me).start()
    own_copy = pltpu.make_async_copy(normed_ref, tokens.at[me], own_sem)
    own_copy.start()
    loop(ep_count - 1, lambda turn: rank_copy(ep_at(turn), me).start())
    picks[me] = rank_ref[me]

    def spread_pieces(turn):
        slot = chip_at(turn) * CORES + core
        plane_copy(slot, tp_me, tp_me).wait_recv()
        loop(tp_count - 1, lambda way: plane_copy(slot, tp_me, tp_at(way)).start())

    def share_blocks(turn):
        slot = chip_at(turn) * CORES + core
        loop(tp_count - 1, lambda way: plane_copy(slot, tp_at(way), tp_me).wait_recv())
        block_copy(tokens.at[slot], slot).start()

    ones = jnp.ones((rows, LANES), jnp.bfloat16)

    def block_step(block, source, first):
        for pair in range(pairs):
            lanes = pl.ds(pair * LANES, LANES)
            value_lanes = pl.ds(width + pair * LANES, LANES)

            def one_tile(index, carry):
                start = pl.multiple_of(index * tile, tile)
                q_rows = pl.ds(start, tile)
                gates = gate_ref[pl.ds(pl.multiple_of(block * rows, rows), rows), lanes]
                keys = jnp.concatenate([source[:, lanes], gates], axis=1)
                values = jnp.concatenate([source[:, value_lanes], ones], axis=1)
                for head in range(2 * pair, min(2 * pair + 2, heads)):
                    scores = lax.dot_general(
                        q_ref[head, q_rows, :],
                        keys,
                        (((1,), (1,)), ((), ())),
                        preferred_element_type=jnp.float32,
                    )
                    if first:
                        q_pos = start + lax.broadcasted_iota(jnp.int32, scores.shape, 0)
                        k_pos = lax.broadcasted_iota(jnp.int32, scores.shape, 1)
                        scores = jnp.where(k_pos <= q_pos, scores, neg_fill)
                        top = jnp.max(scores, axis=1, keepdims=True)
                        new_max = jnp.broadcast_to(top, (tile, LANES))
                    else:
                        old_max = row_max[head, q_rows, :]
                        new_max = jnp.maximum(old_max, jnp.max(scores, axis=1, keepdims=True))
                    probs = jnp.exp(scores - new_max[:, :1]).astype(jnp.bfloat16)
                    add = jnp.dot(probs, values, preferred_element_type=jnp.float32)
                    if not first:
                        keep = jnp.exp(old_max - new_max)
                        add = add + acc[head, q_rows, :] * jnp.concatenate([keep, keep], axis=1)
                    acc[head, q_rows, :] = add
                    row_max[head, q_rows, :] = new_max
                return carry

            lax.fori_loop(0, tiles, one_tile, 0)

    block_step(me, kv_ref, True)
    loop(chips - 1, spread_pieces)

    @pl.when(me == 0)
    def _():
        loop(chips - 1, share_blocks)

    def remote_step(step, carry):
        turn = step - core + 2
        own_core = turn % 2 == 0
        order = turn // 2
        back = jnp.where(order < 2, order, chip + 2 - order)
        slot = (chip - back) * CORES + jnp.where(own_core, core, other)
        landed = held.at[slot]
        side_copy(landed, slot).wait_recv()

        @pl.when(jnp.logical_and(own_core, jnp.logical_and(chip < chips - 1, back < reach)))
        def _():
            up_copy(landed, slot).start()

        @pl.when(own_core)
        def _():
            side_copy(landed, slot).start()

        @pl.when(step == jnp.maximum(me - 2, 0))
        def _():
            loop(chips - 1, share_blocks)

        block_step(slot, landed, False)
        return carry

    lax.fori_loop(0, me, remote_step, 0)

    for head in range(heads):
        pair, part = head // 2, head % 2
        spot = slice(part * HEAD, part * HEAD + HEAD)
        whole = acc[head, :, :LANES] / acc[head, :, LANES:]
        out_ref[:, head * HEAD : (head + 1) * HEAD] = whole[:, spot].astype(out_ref.dtype)

    def finish(step):
        slot = (chip - step) * CORES + core

        @pl.when(jnp.logical_and(chip < chips - 1, step < reach))
        def _():
            up_copy(held.at[slot], slot).wait_send()

        @pl.when(step > 0)
        def _():
            side_copy(held.at[slot], slot).wait_send()

    loop(chip + 1, finish)
    loop(far_count, lambda turn: far_copy(chips - 1 - turn).wait_send())

    @pl.when(core == 0)
    def _():
        side_copy(kv_ref, me).wait_send()

    def finish_tokens(turn):
        target = chip_at(turn)
        slot = target * CORES + core
        chip_copy(target).wait_send()
        loop(tp_count - 1, lambda way: plane_copy(slot, tp_me, tp_at(way)).wait_send())
        block_copy(tokens.at[slot], slot).wait_send()

    loop(chips - 1, finish_tokens)
    block_copy(normed_ref, me).wait_send()

    def finish_blocks(index):
        slot = index * CORES + other
        block_copy(tokens.at[slot], slot).wait_recv()

    loop(chips, finish_blocks)
    own_copy.wait()

    def finish_ranks(turn):
        rank_copy(ep_at(turn), me).wait_send()
        rank_copy(ep_at(turn), ep_at(turn)).wait_recv()

    loop(ep_count - 1, finish_ranks)


def exchange_kernel(count, *refs):
    sources, targets = refs[:count], refs[count : 2 * count]
    send_sem, recv_sem, own_sem = refs[2 * count :]
    tp_count = lax.axis_size("tp")
    tp_me = lax.axis_index("tp")
    barrier = pltpu.get_barrier_semaphore()
    ways = [lax.rem(tp_me + turn, tp_count) for turn in range(1, tp_count)]
    for way in ways:
        pl.semaphore_signal(barrier, inc=1, device_id={"tp": way})
    pl.semaphore_wait(barrier, tp_count - 1)

    def place(index, owner):
        span = sources[index].shape[1]
        if span % LANES:
            return targets[index].at[owner]
        return targets[index].at[:, pl.ds(pl.multiple_of(owner * span, span), span)]

    def copy(index, way, owner):
        return pltpu.make_async_remote_copy(
            src_ref=sources[index],
            dst_ref=place(index, owner),
            send_sem=send_sem.at[index, way],
            recv_sem=recv_sem.at[index, owner],
            device_id={"tp": way},
        )

    for index in range(count):
        for way in ways:
            copy(index, way, tp_me).start()
    own = [
        pltpu.make_async_copy(sources[index], place(index, tp_me), own_sem.at[index])
        for index in range(count)
    ]
    for one in own:
        one.start()
    for one in own:
        one.wait()
    for index in range(count):
        for way in ways:
            copy(index, way, way).wait_recv()
            copy(index, way, tp_me).wait_send()


def exchange(collective_id, *arrays):
    tp_count = lax.axis_size("tp")
    count = len(arrays)

    def gathered(a):
        rows, span = a.shape
        shape = (tp_count, rows, span) if span % LANES else (rows, tp_count * span)
        return jax.ShapeDtypeStruct(shape, a.dtype)

    results = pl.pallas_call(
        functools.partial(exchange_kernel, count),
        out_shape=[gathered(a) for a in arrays],
        in_specs=[pl.BlockSpec(memory_space=pltpu.VMEM)] * count,
        out_specs=[pl.BlockSpec(memory_space=pltpu.VMEM)] * count,
        scratch_shapes=[
            pltpu.SemaphoreType.DMA((count, tp_count)),
            pltpu.SemaphoreType.DMA((count, tp_count)),
            pltpu.SemaphoreType.DMA((count,)),
        ],
        compiler_params=pltpu.CompilerParams(collective_id=collective_id, has_side_effects=True),
        cost_estimate=pl.CostEstimate(flops=0, bytes_accessed=24 * 1024 * 1024, transcendentals=0),
        name="exchange",
    )(*arrays)
    return [
        r if r.ndim == 2 else r.transpose(1, 0, 2).reshape(r.shape[1], -1) for r in results
    ]


def attention(query_rows, key_rows, value_rows, cum_gate, normed, ranks):
    rows, width = query_rows.shape
    heads = width // HEAD
    pairs = (heads + 1) // 2
    ep_count = lax.axis_size("ep")
    padded = pairs * LANES
    if padded > width:
        spare = ((0, 0), (0, padded - width))
        query_rows, key_rows, value_rows = (
            jnp.pad(a, spare) for a in (query_rows, key_rows, value_rows)
        )
    key_value = jnp.concatenate([key_rows, value_rows], axis=1)
    scaled = query_rows * jnp.asarray(HEAD**-0.5, jnp.bfloat16)
    lane = jnp.arange(LANES)
    parts = []
    for head in range(heads):
        pair, part = head // 2, head % 2
        piece = scaled[:, pair * LANES : (pair + 1) * LANES]
        piece = jnp.where((lane // HEAD == part)[None], piece, 0)
        marks = ((lane // 3) == part).astype(jnp.bfloat16)
        parts.append(jnp.concatenate([piece, jnp.broadcast_to(marks, (rows, LANES))], axis=1))
    queries = jnp.stack(parts)
    minus = -cum_gate
    high = lax.reduce_precision(minus, 8, 7)
    rest = minus - high
    mid = lax.reduce_precision(rest, 8, 7)
    low = rest - mid
    terms = jnp.concatenate([high, mid, low], axis=0).astype(jnp.bfloat16)
    source = jnp.arange(3 * heads)
    spot = (source % heads // 2) * LANES + (source % heads % 2) * 3 + source // heads
    layout = (spot[:, None] == jnp.arange(padded)[None, :]).astype(jnp.bfloat16)
    gates = lax.dot_general(
        terms, layout, (((0,), (0,)), ((), ())), preferred_element_type=jnp.float32
    ).astype(jnp.bfloat16)
    blocks = ep_count * rows * rows * heads
    return pl.pallas_call(
        functools.partial(attention_kernel, heads),
        out_shape=[
            jax.ShapeDtypeStruct((rows, heads * HEAD), jnp.bfloat16),
            jax.ShapeDtypeStruct((ep_count,) + normed.shape, jnp.bfloat16),
            jax.ShapeDtypeStruct(ranks.shape, jnp.bfloat16),
        ],
        in_specs=[pl.BlockSpec(memory_space=pltpu.VMEM)] * 5,
        out_specs=[
            pl.BlockSpec(memory_space=pltpu.VMEM),
            pl.BlockSpec(memory_space=pl.ANY),
            pl.BlockSpec(memory_space=pltpu.VMEM),
        ],
        scratch_shapes=[
            pltpu.VMEM((ep_count, rows, 2 * padded), jnp.bfloat16),
            pltpu.VMEM((heads, rows, 2 * LANES), jnp.float32),
            pltpu.VMEM((heads, rows, LANES), jnp.float32),
            pltpu.SemaphoreType.DMA((ep_count,)),
            pltpu.SemaphoreType.DMA((ep_count,)),
            pltpu.SemaphoreType.DMA((ep_count,)),
            pltpu.SemaphoreType.DMA((ep_count,)),
            pltpu.SemaphoreType.DMA((ep_count, lax.axis_size("tp"))),
            pltpu.SemaphoreType.DMA((ep_count, lax.axis_size("tp"))),
            pltpu.SemaphoreType.DMA((ep_count,)),
            pltpu.SemaphoreType.DMA((ep_count,)),
            pltpu.SemaphoreType.DMA,
            pltpu.SemaphoreType.DMA((ep_count,)),
            pltpu.SemaphoreType.DMA((ep_count,)),
        ],
        compiler_params=pltpu.CompilerParams(
            collective_id=0, has_side_effects=True, vmem_limit_bytes=48 * 1024 * 1024
        ),
        cost_estimate=pl.CostEstimate(
            flops=blocks * 2 * 512, bytes_accessed=8 * 1024 * 1024, transcendentals=blocks
        ),
        name="attend",
    )(queries, key_value, gates, normed, ranks)


def local(
    query_rows,
    key_rows,
    value_rows,
    cum_gate,
    out_weight,
    moe_input,
    moe_gain,
    routes,
    route_weight,
    expert_gate,
    expert_up,
    expert_down,
    shared_gate,
    shared_up,
    shared_down,
):
    token_count = moe_input.shape[0]
    top_count = routes.shape[1]
    local_experts = expert_gate.shape[0]
    ep_count = lax.axis_size("ep")
    expert_count = local_experts * ep_count
    capacity = 2 * token_count * top_count // expert_count
    column_count = expert_down.shape[2]
    first_column = lax.axis_index("tp") * column_count
    moe_rows = moe_input.astype(jnp.float32)
    normed = (
        moe_rows
        * lax.rsqrt(jnp.mean(moe_rows * moe_rows, axis=1, keepdims=True) + norm_eps)
        * moe_gain
    ).astype(jnp.bfloat16)
    expert_ids = jnp.arange(expert_count, dtype=jnp.int32)
    chosen = routes[:, :, None] == expert_ids[None, None, :]
    named = jnp.any(chosen, axis=1)
    weight_of = jnp.sum(jnp.where(chosen, route_weight[:, :, None], 0.0), axis=1)
    order = jnp.arange(token_count)
    earlier = (order[None, :] < order[:, None]).astype(jnp.bfloat16)
    ranks = jnp.dot(earlier, named.astype(jnp.bfloat16), preferred_element_type=jnp.float32)
    ranks = jnp.where(named, ranks.astype(jnp.int32), -1)
    slots = jnp.arange(capacity, dtype=jnp.int32)
    place = ranks[:, :, None] == slots[None, None, :]
    rank_rows = ranks.astype(jnp.bfloat16).T.reshape(ep_count, local_experts, token_count)
    heads_out, tokens, mine = attention(
        query_rows, key_rows, value_rows, cum_gate, normed, rank_rows
    )
    pick = mine[:, :, None, :] == slots.astype(jnp.bfloat16)[None, None, :, None]
    pick = pick.astype(jnp.bfloat16).reshape(ep_count, local_experts * capacity, token_count)
    arrived = jnp.einsum("ast,atd->asd", pick, tokens, preferred_element_type=jnp.float32)
    arrived = arrived.astype(jnp.bfloat16).reshape(ep_count, local_experts, capacity, -1)
    gate_val = jnp.einsum(
        "aecd,edf->aecf", arrived, expert_gate, preferred_element_type=jnp.float32
    )
    up_val = jnp.einsum("aecd,edf->aecf", arrived, expert_up, preferred_element_type=jnp.float32)
    hidden = (jax.nn.silu(gate_val) * up_val).astype(jnp.bfloat16)
    shared_hidden = (
        jax.nn.silu(jnp.dot(normed, shared_gate, preferred_element_type=jnp.float32))
        * jnp.dot(normed, shared_up, preferred_element_type=jnp.float32)
    ).astype(jnp.bfloat16)
    slot_count = ep_count * local_experts * capacity
    by_expert = hidden.transpose(1, 0, 2, 3).reshape(slot_count, hidden.shape[3])
    hidden, shared_all = exchange(1, by_expert, shared_hidden)
    hidden = hidden.reshape(local_experts, ep_count * capacity, -1)
    result = jnp.einsum("esf,efd->esd", hidden, expert_down, preferred_element_type=jnp.float32)
    result = result.astype(jnp.bfloat16).reshape(local_experts, ep_count, capacity, column_count)
    result = result.transpose(1, 0, 2, 3)
    result, heads_out = lax.optimization_barrier((result, heads_out))
    returned = lax.all_to_all(result, "ep", split_axis=0, concat_axis=0, tiled=True)
    returned = returned.reshape(expert_count * capacity, column_count)
    weight_high = lax.reduce_precision(weight_of, 8, 7)
    weight_low = weight_of - weight_high
    routed = 0.0
    for weight in (weight_high, weight_low):
        spread = jnp.where(place, weight[:, :, None], 0.0).astype(jnp.bfloat16)
        routed = routed + jnp.dot(
            spread.reshape(token_count, expert_count * capacity),
            returned,
            preferred_element_type=jnp.float32,
        )
    (heads_all,) = exchange(2, heads_out)
    mixer_sum = jnp.dot(heads_all, out_weight, preferred_element_type=jnp.float32)
    moe_total = routed + jnp.dot(shared_all, shared_down, preferred_element_type=jnp.float32)
    return (mixer_sum.astype(jnp.bfloat16), moe_total.astype(jnp.bfloat16))


def solution(mesh):
    placed = (
        P("ep", "tp"),
        P("ep", "tp"),
        P("ep", "tp"),
        P("tp", None),
        P(None, "tp"),
        P("ep", None),
        P(),
        P("ep", None),
        P("ep", None),
        P("ep", None, "tp"),
        P("ep", None, "tp"),
        P("ep", None, "tp"),
        P(None, "tp"),
        P(None, "tp"),
        P(None, "tp"),
    )
    return jax.shard_map(
        local, mesh=mesh, in_specs=placed, out_specs=(P("ep", "tp"), P("ep", "tp")), check_vma=False
    )
```

profile of v0, /device:TPU:25, one launch (start us, length us, event | category | flops | bytes accessed | tf_op | source)
XLA Modules:
  0.0 181.7 jit_solution(2117989106883149727)
XLA Ops:
  0.6 0.0 copy-start
  0.6 0.0 copy-start.3
  0.7 0.0 copy-start.7
  0.7 0.0 copy-start.8
  0.8 1.2 broadcast_multiply_fusion
  2.0 1.0 reduce-precision_convert_fusion.1
  2.9 0.0 copy-done.3
  2.9 0.2 fusion.4
  3.2 0.0 copy-done.7
  3.2 0.2 fusion.16
  3.4 0.0 copy-done.8
  3.4 1.4 fusion.6.normed_ref
  4.8 1.2 pad_maximum_fusion.1.kv_ref
  6.0 0.1 broadcast_select_fusion.3
  6.1 0.2 maximum_bitcast_fusion
  6.3 0.2 pad_maximum_fusion.q_ref
  6.5 2.7 %convolution_convert_fusion.gate_ref = bf16[6144,256]{1,0:T(8,128)(2,1)} fusion(bf16[4,6144]{1,0:T(4,128)(2,1)S(1)} %get-tuple-element.23, bf16[4,6144]{1,0:T(4,128)(2,1)S(1)} %get-tuple-element.24, bf16[4,6144]{1,0:T(4,128)(2,1)S(1)} %get-tuple-element.22, s32[12]{0:T(128)S(1)} %fusion.25), kind=kOutput, calls=%fused_computation | convolution fusion | flops 39767040 | bytes 3293232 | tf_op jit(solution)/shard_map/dot_general | solution.py:405
  9.2 88.2 %attend.1 = (bf16[768,256]{1,0:T(8,128)(2,1)S(1)}, bf16[8,192,2048]{2,1,0:T(8,128)(2,1)}, bf16[8,4,192]{2,1,0:T(4,128)(2,1)S(1)}) custom-call(bf16[4,768,256]{2,1,0:T(8,128)(2,1)S(1)} %pad_maximum_fusion.q_ref, bf16[768,512]{1,0:T(8,128)(2,1)S(1)} %pad_maximum_fusion.1.kv_ref, bf16[6144,256]{1,0:T(8,128)(2,1)} %convolution_convert_fusion.gate_ref, ...), custom_call_target="tpu_custom_call" | custom-call | flops 19327352832 | bytes 8388608 | tf_op jit(solution)/shard_map/attend/pallas_call | solution.py:409
  97.5 0.0 copy-start.1
  97.5 0.8 copy-done.1
  98.3 0.1 eq.124
  98.3 0.3 bitcast_compare_fusion
  98.6 4.2 %convolution_convert_fusion.1 = bf16[8,144,2048]{2,1,0:T(8,128)(2,1)S(1)} fusion(bf16[8,192,2048]{2,1,0:T(8,128)(2,1)} %get-tuple-element.10, pred[8,144,192]{2,0,1:T(8,128)(4,1)S(1)} %bitcast_compare_fusion), kind=kOutput, calls=%fused_computation.1 | convolution fusion | flops 908328960 | bytes 11231232 | tf_op jit(solution)/shard_map/ast,atd->asd/dot_general | solution.py:495
  102.8 0.0 copy-start.2
  102.8 2.6 %copy.33 = bf16[8,144,2048]{2,0,1:T(8,128)(2,1)S(1)} copy(bf16[8,144,2048]{2,1,0:T(8,128)(2,1)S(1)} %convolution_convert_fusion.1) | data formatting | bytes 9437184 | tf_op jit(solution)/shard_map/convert_element_type | solution.py:496
  105.4 0.0 copy-done.2
  105.4 0.0 copy-start.10
  105.4 1.4 fusion.2
  106.8 0.2 copy-done.10
  107.0 1.4 fusion.10
  108.4 0.1 copy.34
  108.4 0.8 reshape.191.refs_0_
  109.2 1.4 fusion.29
  110.6 2.0 %fusion.15.refs_1_ = bf16[192,128]{1,0:T(8,128)(2,1)} fusion(bf16[192,2048]{1,0:T(8,128)(2,1)S(1)} %fusion.6.normed_ref, bf16[2048,128]{1,0:T(8,128)(2,1)} %param.28, f32[192,128]{1,0:T(8,128)S(1)} %fusion.29), kind=kOutput, calls=%fused_computation.24 | convolution fusion | flops 100810752 | bytes 1458176 | tf_op jit(solution)/shard_map/dot_general | solution.py:504
  112.6 20.5 %exchange.2 = (bf16[1152,512]{1,0:T(8,128)(2,1)}, bf16[192,512]{1,0:T(8,128)(2,1)}) custom-call(bf16[1152,128]{1,0:T(8,128)(2,1)} %reshape.191.refs_0_, bf16[192,128]{1,0:T(8,128)(2,1)} %fusion.15.refs_1_), custom_call_target="tpu_custom_call" | custom-call | bytes 25165824 | tf_op jit(solution)/shard_map/exchange/pallas_call | solution.py:355
  133.2 0.0 copy-done
  133.2 2.0 %convolution_convert_fusion.2 = bf16[4,288,512]{2,1,0:T(8,128)(2,1)S(1)} fusion(bf16[4,288,512]{2,1,0:T(8,128)(2,1)} %bitcast.56, bf16[4,512,512]{2,1,0:T(8,128)(2,1)S(1)} %copy-done), kind=kOutput, calls=%fused_computation.12 | convolution fusion | flops 604569600 | bytes 4456448 | tf_op jit(solution)/shard_map/esf,efd->esd/dot_general | solution.py:510
  135.2 1.9 %copy.35 = bf16[4,288,512]{2,0,1:T(4,128)(2,1)} copy(bf16[4,288,512]{2,1,0:T(8,128)(2,1)S(1)} %convolution_convert_fusion.2) | data formatting | bytes 2359296 | tf_op jit(solution)/shard_map/convert_element_type | solution.py:511
  137.2 0.0 copy-start.9
  137.2 5.4 %all-to-all-start = ((bf16[8,4,36,512]{3,1,2,0:T(4,128)(2,1)}), bf16[8,4,36,512]{3,1,2,0:T(4,128)(2,1)S(1)}, u32[]{:S(2)}, u32[]{:S(2)}) async-start(bf16[8,4,36,512]{3,1,2,0:T(4,128)(2,1)} %bitcast.55), calls=%async_computation | async-start | bytes 2359296 | tf_op jit(solution)/shard_map/all_to_all | solution.py:514
  142.6 0.0 copy-done.9
  142.6 1.5 select_convert_fusion
  144.1 2.1 %convert_element_type.110 = bf16[192,1152]{0,1:T(8,128)(2,1)} reshape(bf16[192,32,36]{0,2,1:T(8,128)(2,1)} %get-tuple-element.26) | data formatting | bytes 884736 | tf_op jit(solution)/shard_map/convert_element_type | solution.py:520
  146.3 2.1 %convert_element_type.112 = bf16[192,1152]{0,1:T(8,128)(2,1)} reshape(bf16[192,32,36]{0,2,1:T(8,128)(2,1)} %get-tuple-element.25) | data formatting | bytes 884736 | tf_op jit(solution)/shard_map/convert_element_type | solution.py:520
  148.4 22.6 %exchange.3 = bf16[768,1024]{1,0:T(8,128)(2,1)} custom-call(bf16[768,256]{1,0:T(8,128)(2,1)} %copy-done.1), custom_call_target="tpu_custom_call" | custom-call | bytes 25165824 | tf_op jit(solution)/shard_map/exchange/pallas_call | solution.py:355
  171.0 3.6 %convolution_convert_fusion.3 = bf16[768,512]{1,0:T(8,128)(2,1)} fusion(bf16[768,1024]{1,0:T(8,128)(2,1)} %exchange.3, bf16[1024,512]{1,0:T(8,128)(2,1)} %param.19), kind=kOutput, calls=%fused_computation.13 | convolution fusion | flops 805699584 | bytes 3407872 | tf_op jit(solution)/shard_map/dot_general | solution.py:527
  174.6 0.0 all-to-all-done
  174.6 1.4 copy.36
  175.9 2.1 %reshape.194 = bf16[1152,512]{1,0:T(8,128)(2,1)S(1)} reshape(bf16[8,4,36,512]{3,2,1,0:T(8,128)(2,1)} %copy.36) | data formatting | bytes 2359296 | tf_op jit(solution)/shard_map/reshape | solution.py:515
  178.1 0.0 copy-start.4
  178.1 1.6 fusion.30
  179.7 0.0 copy-done.4
  179.7 0.0 copy-start.5
  179.7 0.0 copy-start.6
  179.7 0.4 convolution_add_fusion.1
  180.1 0.6 copy-done.5
  180.7 0.0 copy-done.6
  180.8 1.0 fusion.14
  (16 shorter events, 0.2 us)
Async XLA Ops:
  0.6 132.6 %copy-start = (bf16[4,512,512]{2,1,0:T(8,128)(2,1)S(1)}, bf16[4,512,512]{2,1,0:T(8,128)(2,1)}, u32[]{:S(2)}) copy-start(bf16[4,512,512]{2,1,0:T(8,128)(2,1)} %param.26) | copy-start | bytes 6291460
  0.6 2.3 %copy-start.3 = (bf16[192,2048]{1,0:T(8,128)(2,1)S(1)}, bf16[192,2048]{1,0:T(8,128)(2,1)}, u32[]{:S(2)}) copy-start(bf16[192,2048]{1,0:T(8,128)(2,1)} %param.20) | copy-start | bytes 2359300
  0.7 2.5 %copy-start.7 = (s32[192,3]{0,1:T(4,128)S(1)}, s32[192,3]{0,1:T(4,128)}, u32[]{:S(2)}) copy-start(s32[192,3]{0,1:T(4,128)} %param.22) | copy-start | bytes 6916
  0.7 2.8 %copy-start.8 = (f32[2048]{0:T(1024)S(1)}, f32[2048]{0:T(1024)}, u32[]{:S(2)}) copy-start(f32[2048]{0:T(1024)} %param.21) | copy-start | bytes 24580
  97.5 0.8 copy-start.1
  102.8 2.6 %copy-start.2 = (bf16[4,2048,128]{2,1,0:T(8,128)(2,1)S(1)}, bf16[4,2048,128]{2,1,0:T(8,128)(2,1)}, u32[]{:S(2)}) copy-start(bf16[4,2048,128]{2,1,0:T(8,128)(2,1)} %param.24) | copy-start | bytes 6291460
  105.4 1.6 copy-start.10
  137.2 5.4 %copy-start.9 = (f32[192,3]{0,1:T(4,128)S(1)}, f32[192,3]{0,1:T(4,128)}, u32[]{:S(2)}) copy-start(f32[192,3]{0,1:T(4,128)} %param.23) | copy-start | bytes 6916
  137.2 37.4 %all-to-all-start = ((bf16[8,4,36,512]{3,1,2,0:T(4,128)(2,1)}), bf16[8,4,36,512]{3,1,2,0:T(4,128)(2,1)S(1)}, u32[]{:S(2)}, u32[]{:S(2)}) async-start(bf16[8,4,36,512]{3,1,2,0:T(4,128)(2,1)} %bitcast.55), calls=%async_computation | async-start | bytes 2359296 | tf_op jit(solution)/shard_map/all_to_all | solution.py:514
  178.1 1.6 copy-start.4
  179.7 1.0 copy-start.5
  179.7 1.1 copy-start.6
where the time goes:
time: 184 us; the launch traced here: 182 us
  Pallas kernels  131 us (71%)
  matrix products  21.8 us (12%)
  local copies, waits for them, and re-layouts  14.8 us (8%)
  other arithmetic  7.29 us (4%)
  starting transfers between devices  5.4 us (3%)
    pallas_call x1, Pallas kernels, attention(): pl.pallas_call(functools.partial(attention_kernel, heads), out_shape=[jax...  88.2 us
    pallas_call x2, Pallas kernels, exchange(): pl.pallas_call(functools.partial(exchange_kernel, count), out_shape=[gath...  43.1 us
    all_to_all x1, starting transfers between devices, local(): lax.all_to_all(result, 'ep', split_axis=0, concat_axis=0, tiled=True)  5.4 us
    convert_element_type x2, local copies, waits for them, and re-layouts, local(): spread = jnp.where(place, weight[:, :, None], 0.0).astype(jnp.bfloat16)  4.24 us
    dot_general x1, matrix products, local(): jnp.einsum('ast,atd->asd', pick, tokens, preferred_element_type=jnp.float32)  4.17 us
  transfers between devices with their start and end apart: 1, of which 0 were waited for; matrix products, arithmetic and copies ran while one was open for 5% of the time, Pallas kernels for 12%

commit v1 on v0

--- a/solution.py
+++ b/solution.py
@@ -28,6 +28,10 @@
     held,
     acc,
     row_max,
+    scores_even,
+    scores_odd,
+    tops_even,
+    tops_odd,
     up_send,
     side_send,
     recv_sem,
@@ -43,8 +47,9 @@
     rows = kv_ref.shape[0]
     width = kv_ref.shape[1] // 2
     pairs = width // LANES
-    tile = 256 if rows % 256 == 0 else rows
+    tile = tops_even.shape[0]
     tiles = rows // tile
+    scores, tops = (scores_even, scores_odd), (tops_even, tops_odd)
     me = lax.axis_index("ep")
     chips = lax.axis_size("ep") // CORES
     chip = me // CORES
@@ -179,45 +184,54 @@
         loop(tp_count - 1, lambda way: plane_copy(slot, tp_at(way), tp_me).wait_recv())
         block_copy(tokens.at[slot], slot).start()
 
-    ones = jnp.ones((rows, LANES), jnp.bfloat16)
+    units = [(head, index) for head in range(heads) for index in range(tiles)]
+    lane = lax.broadcasted_iota(jnp.int32, (rows, LANES), 1)
+
+    def score_unit(block, source, first, unit, slot):
+        head, index = unit
+        pair = head // 2
+        lanes = pl.ds(pair * LANES, LANES)
+        span = (index + 1) * tile if first else rows
+        gates = gate_ref[pl.ds(pl.multiple_of(block * rows, rows), span), lanes]
+        keys = jnp.concatenate([source[:span, lanes], gates], axis=1)
+        result = lax.dot_general(
+            q_ref[head, index * tile : (index + 1) * tile, :],
+            keys,
+            (((1,), (1,)), ((), ())),
+            preferred_element_type=jnp.float32,
+        )
+        if first:
+            q_pos = index * tile + lax.broadcasted_iota(jnp.int32, result.shape, 0)
+            k_pos = lax.broadcasted_iota(jnp.int32, result.shape, 1)
+            result = jnp.where(k_pos <= q_pos, result, neg_fill)
+        scores[slot][:, :span] = result
+        tops[slot][...] = jnp.broadcast_to(jnp.max(result, axis=1, keepdims=True), (tile, LANES))
+
+    def value_unit(source, first, unit, slot):
+        head, index = unit
+        pair, part = head // 2, head % 2
+        q_rows = slice(index * tile, (index + 1) * tile)
+        span = (index + 1) * tile if first else rows
+        new_max = tops[slot][...]
+        if not first:
+            old_max = row_max[head, q_rows, :]
+            new_max = jnp.maximum(old_max, new_max)
+        wide = jnp.concatenate([new_max] * (span // LANES), axis=1)
+        probs = jnp.exp(scores[slot][:, :span] - wide).astype(jnp.bfloat16)
+        values = source[:span, pl.ds(width + pair * LANES, LANES)]
+        values = jnp.where(lane[:span] // HEAD == part, values, jnp.ones_like(values))
+        add = jnp.dot(probs, values, preferred_element_type=jnp.float32)
+        if not first:
+            add = add + acc[head, q_rows, :] * jnp.exp(old_max - new_max)
+        acc[head, q_rows, :] = add
+        row_max[head, q_rows, :] = new_max
 
     def block_step(block, source, first):
-        for pair in range(pairs):
-            lanes = pl.ds(pair * LANES, LANES)
-            value_lanes = pl.ds(width + pair * LANES, LANES)
-
-            def one_tile(index, carry):
-                start = pl.multiple_of(index * tile, tile)
-                q_rows = pl.ds(start, tile)
-                gates = gate_ref[pl.ds(pl.multiple_of(block * rows, rows), rows), lanes]
-                keys = jnp.concatenate([source[:, lanes], gates], axis=1)
-                values = jnp.concatenate([source[:, value_lanes], ones], axis=1)
-                for head in range(2 * pair, min(2 * pair + 2, heads)):
-                    scores = lax.dot_general(
-                        q_ref[head, q_rows, :],
-                        keys,
-                        (((1,), (1,)), ((), ())),
-                        preferred_element_type=jnp.float32,
-                    )
-                    if first:
-                        q_pos = start + lax.broadcasted_iota(jnp.int32, scores.shape, 0)
-                        k_pos = lax.broadcasted_iota(jnp.int32, scores.shape, 1)
-                        scores = jnp.where(k_pos <= q_pos, scores, neg_fill)
-                        top = jnp.max(scores, axis=1, keepdims=True)
-                        new_max = jnp.broadcast_to(top, (tile, LANES))
-                    else:
-                        old_max = row_max[head, q_rows, :]
-                        new_max = jnp.maximum(old_max, jnp.max(scores, axis=1, keepdims=True))
-                    probs = jnp.exp(scores - new_max[:, :1]).astype(jnp.bfloat16)
-                    add = jnp.dot(probs, values, preferred_element_type=jnp.float32)
-                    if not first:
-                        keep = jnp.exp(old_max - new_max)
-                        add = add + acc[head, q_rows, :] * jnp.concatenate([keep, keep], axis=1)
-                    acc[head, q_rows, :] = add
-                    row_max[head, q_rows, :] = new_max
-                return carry
-
-            lax.fori_loop(0, tiles, one_tile, 0)
+        score_unit(block, source, first, units[0], 0)
+        for turn, unit in enumerate(units):
+            if turn + 1 < len(units):
+                score_unit(block, source, first, units[turn + 1], (turn + 1) % 2)
+            value_unit(source, first, unit, turn % 2)
 
     block_step(me, kv_ref, True)
     loop(chips - 1, spread_pieces)
@@ -252,11 +266,17 @@
 
     lax.fori_loop(0, me, remote_step, 0)
 
-    for head in range(heads):
-        pair, part = head // 2, head % 2
-        spot = slice(part * HEAD, part * HEAD + HEAD)
-        whole = acc[head, :, :LANES] / acc[head, :, LANES:]
-        out_ref[:, head * HEAD : (head + 1) * HEAD] = whole[:, spot].astype(out_ref.dtype)
+    for pair in range(pairs):
+        members = []
+        for head in range(2 * pair, min(2 * pair + 2, heads)):
+            whole = acc[head]
+            members.append(whole / pltpu.roll(whole, HEAD, 1))
+        joined = members[0]
+        if len(members) > 1:
+            joined = jnp.where(lane < HEAD, members[0], members[1])
+        count = HEAD * len(members)
+        spot = slice(pair * LANES, pair * LANES + count)
+        out_ref[:, spot] = joined[:, :count].astype(out_ref.dtype)
 
     def finish(step):
         slot = (chip - step) * CORES + core
@@ -377,6 +397,7 @@
     pairs = (heads + 1) // 2
     ep_count = lax.axis_size("ep")
     padded = pairs * LANES
+    tile = rows // 2 if rows % (2 * LANES) == 0 else rows
     if padded > width:
         spare = ((0, 0), (0, padded - width))
         query_rows, key_rows, value_rows = (
@@ -421,8 +442,12 @@
         ],
         scratch_shapes=[
             pltpu.VMEM((ep_count, rows, 2 * padded), jnp.bfloat16),
-            pltpu.VMEM((heads, rows, 2 * LANES), jnp.float32),
             pltpu.VMEM((heads, rows, LANES), jnp.float32),
+            pltpu.VMEM((heads, rows, LANES), jnp.float32),
+            pltpu.VMEM((tile, rows), jnp.float32),
+            pltpu.VMEM((tile, rows), jnp.float32),
+            pltpu.VMEM((tile, LANES), jnp.float32),
+            pltpu.VMEM((tile, LANES), jnp.float32),
             pltpu.SemaphoreType.DMA((ep_count,)),
             pltpu.SemaphoreType.DMA((ep_count,)),
             pltpu.SemaphoreType.DMA((ep_count,)),

time: 184 us -> 178 us (0.967)
  Pallas kernels: 131 us -> 125 us
    pallas_call x1, Pallas kernels: 88.2 us -> 81.8 us  [attention(): pl.pallas_call(functools.partial(attention_kernel, heads), out_shape=[jax...]
  transfers between devices with their start and end apart: 1 -> 1, of which waited for: 0 -> 0; matrix products, arithmetic and copies ran while one was open for 5% -> 5% of each run, Pallas kernels for 12% -> 13%
where the time goes in v1:
time: 178 us; the launch traced here: 175 us
  Pallas kernels  125 us (70%)
  matrix products  21.8 us (12%)
  local copies, waits for them, and re-layouts  14.8 us (8%)
  other arithmetic  7.29 us (4%)
  starting transfers between devices  5.4 us (3%)
    pallas_call x1, Pallas kernels, attention(): pl.pallas_call(functools.partial(attention_kernel, heads), out_shape=[jax...  81.8 us
    pallas_call x2, Pallas kernels, exchange(): pl.pallas_call(functools.partial(exchange_kernel, count), out_shape=[gath...  43.1 us
    all_to_all x1, starting transfers between devices, local(): lax.all_to_all(result, 'ep', split_axis=0, concat_axis=0, tiled=True)  5.4 us
    convert_element_type x2, local copies, waits for them, and re-layouts, local(): spread = jnp.where(place, weight[:, :, None], 0.0).astype(jnp.bfloat16)  4.24 us
    dot_general x1, matrix products, local(): jnp.einsum('ast,atd->asd', pick, tokens, preferred_element_type=jnp.float32)  4.16 us
  transfers between devices with their start and end apart: 1, of which 0 were waited for; matrix products, arithmetic and copies ran while one was open for 5% of the time, Pallas kernels for 13%

profile of v1, /device:TPU:25, one launch (start us, length us, event | category | flops | bytes accessed | tf_op | source)
XLA Modules:
  0.0 175.3 jit_solution(8703777118205926316)
XLA Ops:
  0.6 0.0 copy-start
  0.6 0.0 copy-start.3
  0.7 0.0 copy-start.7
  0.7 0.0 copy-start.8
  0.8 1.2 broadcast_multiply_fusion
  2.0 1.0 reduce-precision_convert_fusion.1
  2.9 0.0 copy-done.3
  2.9 0.2 fusion.4
  3.2 0.0 copy-done.7
  3.2 0.2 fusion.16
  3.4 0.0 copy-done.8
  3.4 1.4 fusion.6.normed_ref
  4.8 1.2 pad_maximum_fusion.1.kv_ref
  6.0 0.1 broadcast_select_fusion.3
  6.1 0.2 maximum_bitcast_fusion
  6.3 0.2 pad_maximum_fusion.q_ref
  6.5 2.7 %convolution_convert_fusion.gate_ref = bf16[6144,256]{1,0:T(8,128)(2,1)} fusion(bf16[4,6144]{1,0:T(4,128)(2,1)S(1)} %get-tuple-element.23, bf16[4,6144]{1,0:T(4,128)(2,1)S(1)} %get-tuple-element.24, bf16[4,6144]{1,0:T(4,128)(2,1)S(1)} %get-tuple-element.22, s32[12]{0:T(128)S(1)} %fusion.25), kind=kOutput, calls=%fused_computation | convolution fusion | flops 39767040 | bytes 3293232 | tf_op jit(solution)/shard_map/dot_general | solution.py:426
  9.2 81.8 %attend.1 = (bf16[768,256]{1,0:T(8,128)(2,1)S(1)}, bf16[8,192,2048]{2,1,0:T(8,128)(2,1)}, bf16[8,4,192]{2,1,0:T(4,128)(2,1)S(1)}) custom-call(bf16[4,768,256]{2,1,0:T(8,128)(2,1)S(1)} %pad_maximum_fusion.q_ref, bf16[768,512]{1,0:T(8,128)(2,1)S(1)} %pad_maximum_fusion.1.kv_ref, bf16[6144,256]{1,0:T(8,128)(2,1)} %convolution_convert_fusion.gate_ref, ...), custom_call_target="tpu_custom_call" | custom-call | flops 19327352832 | bytes 8388608 | tf_op jit(solution)/shard_map/attend/pallas_call | solution.py:430
  91.1 0.0 copy-start.1
  91.1 0.8 copy-done.1
  91.8 0.1 eq.124
  91.9 0.3 bitcast_compare_fusion
  92.2 4.2 %convolution_convert_fusion.1 = bf16[8,144,2048]{2,1,0:T(8,128)(2,1)S(1)} fusion(bf16[8,192,2048]{2,1,0:T(8,128)(2,1)} %get-tuple-element.10, pred[8,144,192]{2,0,1:T(8,128)(4,1)S(1)} %bitcast_compare_fusion), kind=kOutput, calls=%fused_computation.1 | convolution fusion | flops 908328960 | bytes 11231232 | tf_op jit(solution)/shard_map/ast,atd->asd/dot_general | solution.py:520
  96.3 0.0 copy-start.2
  96.4 2.6 %copy.33 = bf16[8,144,2048]{2,0,1:T(8,128)(2,1)S(1)} copy(bf16[8,144,2048]{2,1,0:T(8,128)(2,1)S(1)} %convolution_convert_fusion.1) | data formatting | bytes 9437184 | tf_op jit(solution)/shard_map/convert_element_type | solution.py:521
  99.0 0.0 copy-done.2
  99.0 0.0 copy-start.10
  99.0 1.4 fusion.2
  100.4 0.2 copy-done.10
  100.6 1.4 fusion.10
  102.0 0.1 copy.34
  102.0 0.8 reshape.191.refs_0_
  102.8 1.4 fusion.29
  104.2 2.0 %fusion.15.refs_1_ = bf16[192,128]{1,0:T(8,128)(2,1)} fusion(bf16[192,2048]{1,0:T(8,128)(2,1)S(1)} %fusion.6.normed_ref, bf16[2048,128]{1,0:T(8,128)(2,1)} %param.28, f32[192,128]{1,0:T(8,128)S(1)} %fusion.29), kind=kOutput, calls=%fused_computation.24 | convolution fusion | flops 100810752 | bytes 1458176 | tf_op jit(solution)/shard_map/dot_general | solution.py:529
  106.2 20.5 %exchange.2 = (bf16[1152,512]{1,0:T(8,128)(2,1)}, bf16[192,512]{1,0:T(8,128)(2,1)}) custom-call(bf16[1152,128]{1,0:T(8,128)(2,1)} %reshape.191.refs_0_, bf16[192,128]{1,0:T(8,128)(2,1)} %fusion.15.refs_1_), custom_call_target="tpu_custom_call" | custom-call | bytes 25165824 | tf_op jit(solution)/shard_map/exchange/pallas_call | solution.py:375
  126.8 0.0 copy-done
  126.8 2.0 %convolution_convert_fusion.2 = bf16[4,288,512]{2,1,0:T(8,128)(2,1)S(1)} fusion(bf16[4,288,512]{2,1,0:T(8,128)(2,1)} %bitcast.56, bf16[4,512,512]{2,1,0:T(8,128)(2,1)S(1)} %copy-done), kind=kOutput, calls=%fused_computation.12 | convolution fusion | flops 604569600 | bytes 4456448 | tf_op jit(solution)/shard_map/esf,efd->esd/dot_general | solution.py:535
  128.8 1.9 %copy.35 = bf16[4,288,512]{2,0,1:T(4,128)(2,1)} copy(bf16[4,288,512]{2,1,0:T(8,128)(2,1)S(1)} %convolution_convert_fusion.2) | data formatting | bytes 2359296 | tf_op jit(solution)/shard_map/convert_element_type | solution.py:536
  130.8 0.0 copy-start.9
  130.8 5.4 %all-to-all-start = ((bf16[8,4,36,512]{3,1,2,0:T(4,128)(2,1)}), bf16[8,4,36,512]{3,1,2,0:T(4,128)(2,1)S(1)}, u32[]{:S(2)}, u32[]{:S(2)}) async-start(bf16[8,4,36,512]{3,1,2,0:T(4,128)(2,1)} %bitcast.55), calls=%async_computation | async-start | bytes 2359296 | tf_op jit(solution)/shard_map/all_to_all | solution.py:539
  136.2 0.0 copy-done.9
  136.2 1.5 select_convert_fusion
  137.7 2.1 %convert_element_type.110 = bf16[192,1152]{0,1:T(8,128)(2,1)} reshape(bf16[192,32,36]{0,2,1:T(8,128)(2,1)} %get-tuple-element.26) | data formatting | bytes 884736 | tf_op jit(solution)/shard_map/convert_element_type | solution.py:545
  139.8 2.1 %convert_element_type.112 = bf16[192,1152]{0,1:T(8,128)(2,1)} reshape(bf16[192,32,36]{0,2,1:T(8,128)(2,1)} %get-tuple-element.25) | data formatting | bytes 884736 | tf_op jit(solution)/shard_map/convert_element_type | solution.py:545
  142.0 22.6 %exchange.3 = bf16[768,1024]{1,0:T(8,128)(2,1)} custom-call(bf16[768,256]{1,0:T(8,128)(2,1)} %copy-done.1), custom_call_target="tpu_custom_call" | custom-call | bytes 25165824 | tf_op jit(solution)/shard_map/exchange/pallas_call | solution.py:375
  164.6 3.6 %convolution_convert_fusion.3 = bf16[768,512]{1,0:T(8,128)(2,1)} fusion(bf16[768,1024]{1,0:T(8,128)(2,1)} %exchange.3, bf16[1024,512]{1,0:T(8,128)(2,1)} %param.19), kind=kOutput, calls=%fused_computation.13 | convolution fusion | flops 805699584 | bytes 3407872 | tf_op jit(solution)/shard_map/dot_general | solution.py:552
  168.1 0.0 all-to-all-done
  168.1 1.4 copy.36
  169.5 2.1 %reshape.194 = bf16[1152,512]{1,0:T(8,128)(2,1)S(1)} reshape(bf16[8,4,36,512]{3,2,1,0:T(8,128)(2,1)} %copy.36) | data formatting | bytes 2359296 | tf_op jit(solution)/shard_map/reshape | solution.py:540
  171.6 0.0 copy-start.4
  171.7 1.6 fusion.30
  173.2 0.0 copy-done.4
  173.2 0.0 copy-start.5
  173.3 0.0 copy-start.6
  173.3 0.5 convolution_add_fusion.1
  173.7 0.6 copy-done.5
  174.3 0.0 copy-done.6
  174.3 1.0 fusion.14
  (16 shorter events, 0.2 us)
Async XLA Ops:
  0.6 126.1 %copy-start = (bf16[4,512,512]{2,1,0:T(8,128)(2,1)S(1)}, bf16[4,512,512]{2,1,0:T(8,128)(2,1)}, u32[]{:S(2)}) copy-start(bf16[4,512,512]{2,1,0:T(8,128)(2,1)} %param.26) | copy-start | bytes 6291460
  0.6 2.3 %copy-start.3 = (bf16[192,2048]{1,0:T(8,128)(2,1)S(1)}, bf16[192,2048]{1,0:T(8,128)(2,1)}, u32[]{:S(2)}) copy-start(bf16[192,2048]{1,0:T(8,128)(2,1)} %param.20) | copy-start | bytes 2359300
  0.7 2.5 %copy-start.7 = (s32[192,3]{0,1:T(4,128)S(1)}, s32[192,3]{0,1:T(4,128)}, u32[]{:S(2)}) copy-start(s32[192,3]{0,1:T(4,128)} %param.22) | copy-start | bytes 6916
  0.7 2.8 %copy-start.8 = (f32[2048]{0:T(1024)S(1)}, f32[2048]{0:T(1024)}, u32[]{:S(2)}) copy-start(f32[2048]{0:T(1024)} %param.21) | copy-start | bytes 24580
  91.1 0.8 copy-start.1
  96.3 2.6 %copy-start.2 = (bf16[4,2048,128]{2,1,0:T(8,128)(2,1)S(1)}, bf16[4,2048,128]{2,1,0:T(8,128)(2,1)}, u32[]{:S(2)}) copy-start(bf16[4,2048,128]{2,1,0:T(8,128)(2,1)} %param.24) | copy-start | bytes 6291460
  99.0 1.6 copy-start.10
  130.8 5.4 %copy-start.9 = (f32[192,3]{0,1:T(4,128)S(1)}, f32[192,3]{0,1:T(4,128)}, u32[]{:S(2)}) copy-start(f32[192,3]{0,1:T(4,128)} %param.23) | copy-start | bytes 6916
  130.8 37.4 %all-to-all-start = ((bf16[8,4,36,512]{3,1,2,0:T(4,128)(2,1)}), bf16[8,4,36,512]{3,1,2,0:T(4,128)(2,1)S(1)}, u32[]{:S(2)}, u32[]{:S(2)}) async-start(bf16[8,4,36,512]{3,1,2,0:T(4,128)(2,1)} %bitcast.55), calls=%async_computation | async-start | bytes 2359296 | tf_op jit(solution)/shard_map/all_to_all | solution.py:539
  171.6 1.6 copy-start.4
  173.2 1.0 copy-start.5
  173.3 1.1 copy-start.6

commit v2 on v0

v2 whole, which is shorter than its diff:
```python
import functools

import jax
import jax.numpy as jnp
from jax import lax
from jax.experimental import pallas as pl
from jax.experimental.pallas import tpu as pltpu
from jax.sharding import PartitionSpec as P

HEAD = 64
LANES = 128
CORES = 2
ROW_TILE = 16

neg_fill = -1e30
norm_eps = 1e-06


def silu_mul(both):
    gate, up = both[:, :LANES], both[:, LANES:]
    return (gate / (1.0 + jnp.exp(-gate)) * up).astype(jnp.bfloat16)


def block_kernel(
    heads,
    main,
    tail,
    q_hbm,
    k_hbm,
    v_hbm,
    gate_ref,
    normed_ref,
    rank_ref,
    expert_gate,
    expert_up,
    expert_down,
    shared_gate,
    shared_up,
    heads_all,
    returned,
    shared_all,
    tokens,
    q_own,
    q_guest,
    held,
    acc,
    row_max,
    guest_acc,
    guest_max,
    guest_out,
    guest_in,
    guest_lse,
    lse_in,
    scores_even,
    scores_odd,
    tops_even,
    tops_odd,
    picks,
    staged,
    arrived,
    gate_up,
    down,
    shared_both,
    hidden,
    results,
    load_sem,
    up_send,
    side_send,
    kv_recv,
    guest_send,
    guest_recv,
    chip_send,
    plane_send,
    piece_recv,
    block_send,
    block_recv,
    rank_send,
    rank_recv,
    shared_send,
    shared_recv,
    hidden_send,
    hidden_recv,
    heads_send,
    heads_recv,
    result_send,
    result_recv,
    stage_sem,
):
    ep_slots, pairs, _, rows, _ = held.shape
    group = min(2, heads)
    experts = expert_gate.shape[0]
    tile = tops_even.shape[0]
    tiles = rows // tile
    scores, tops = (scores_even, scores_odd), (tops_even, tops_odd)
    me = lax.axis_index("ep")
    ep_count = lax.axis_size("ep")
    chips = ep_count // CORES
    chip = me // CORES
    core = me % CORES
    other = 1 - core
    tp_count = lax.axis_size("tp")
    tp_me = lax.axis_index("tp")
    columns = normed_ref.shape[1] // tp_count
    last = chips - 1
    host = chips - 2
    guests = chips > 2

    barrier = pltpu.get_barrier_semaphore()

    def loop(count, body):
        def step(index, carry):
            body(index)
            return carry

        lax.fori_loop(0, count, step, 0)

    def greet(**where):
        pl.semaphore_signal(barrier, inc=1, device_id=where)

    def chip_at(turn):
        return lax.rem(chip + turn + 1, chips)

    def tp_at(turn):
        return lax.rem(tp_me + turn + 1, tp_count)

    def ep_at(turn):
        return lax.rem(me + turn + 1, ep_count)

    def lanes_at(index, width):
        return pl.ds(pl.multiple_of(index * width, width), width)

    loads = [
        pltpu.make_async_copy(q_hbm, q_own, load_sem.at[0]),
    ]
    for pair in range(pairs):
        lanes = pl.ds(pair * LANES, LANES)
        for part, source in enumerate((k_hbm, v_hbm)):
            loads.append(
                pltpu.make_async_copy(
                    source.at[:, lanes],
                    held.at[me, pair, part],
                    load_sem.at[len(loads)],
                )
            )
    weights = []
    for source, place in (
        (shared_gate, shared_both.at[:, pl.ds(0, LANES)]),
        (shared_up, shared_both.at[:, pl.ds(LANES, LANES)]),
        (expert_gate, gate_up.at[:, :, pl.ds(0, LANES)]),
        (expert_up, gate_up.at[:, :, pl.ds(LANES, LANES)]),
        (expert_down, down),
    ):
        index = len(loads) + len(weights)
        weights.append(pltpu.make_async_copy(source, place, load_sem.at[index]))
    for one in loads + weights:
        one.start()

    loop(ep_count - 1, lambda turn: greet(ep=ep_at(turn)))
    loop(tp_count - 1, lambda turn: greet(tp=tp_at(turn)))
    pl.semaphore_wait(barrier, ep_count + tp_count - 2)

    def remote(source, target, send, recv, **where):
        return pltpu.make_async_remote_copy(
            src_ref=source, dst_ref=target, send_sem=send, recv_sem=recv, device_id=where
        )

    def rank_copy(target, owner):
        return remote(
            rank_ref.at[target], picks.at[owner], rank_send.at[target], rank_recv.at[owner], ep=target
        )

    def up_copy(slot, pair):
        place = held.at[slot, pair]
        return remote(place, place, up_send.at[slot, pair], kv_recv.at[slot, pair], ep=me + CORES)

    def side_copy(slot, pair):
        place = held.at[slot, pair]
        return remote(
            place, place, side_send.at[slot, pair], kv_recv.at[slot, pair], ep=chip * CORES + other
        )

    def guest_query(pair):
        lanes = lanes_at(pair, LANES)
        return remote(
            q_own.at[:, lanes],
            q_guest.at[:, lanes],
            guest_send.at[0, pair],
            guest_recv.at[0, pair],
            ep=me - CORES,
        )

    def guest_result(pair):
        return remote(
            guest_out.at[pair],
            guest_in.at[pair],
            guest_send.at[1, pair],
            guest_recv.at[1, pair],
            ep=me + CORES,
        )

    def guest_stats(pair):
        return remote(
            guest_lse.at[pair],
            lse_in.at[pair],
            guest_send.at[2, pair],
            guest_recv.at[2, pair],
            ep=me + CORES,
        )

    def chip_copy(target):
        return remote(
            normed_ref.at[:, lanes_at(tp_me, columns)],
            tokens.at[me, :, lanes_at(tp_me, columns)],
            chip_send.at[target],
            piece_recv.at[me, tp_me],
            ep=target * CORES + core,
        )

    def plane_copy(slot, piece, target):
        place = tokens.at[slot, :, lanes_at(piece, columns)]
        return remote(
            place, place, plane_send.at[slot, target], piece_recv.at[slot, piece], tp=target
        )

    def block_copy(source, slot):
        return remote(
            source,
            tokens.at[slot],
            block_send.at[slot],
            block_recv.at[slot],
            ep=chip * CORES + other,
        )

    def shared_copy(owner, target):
        place = shared_all.at[owner]
        return remote(place, place, shared_send.at[target], shared_recv.at[owner], tp=target)

    def hidden_copy(owner, target):
        place = hidden.at[owner]
        return remote(place, place, hidden_send.at[target], hidden_recv.at[owner], tp=target)

    wide_heads = heads * HEAD % LANES == 0

    def heads_place(owner, pair):
        if wide_heads:
            return heads_all.at[:, lanes_at(owner * pairs + pair, LANES)]
        return heads_all.at[owner]

    def heads_copy(owner, pair, target):
        place = heads_place(owner, pair)
        return remote(
            place, place, heads_send.at[pair, target], heads_recv.at[pair, owner], tp=target
        )

    def result_copy(target, owner):
        return remote(
            results.at[target],
            returned.at[owner],
            result_send.at[target],
            result_recv.at[owner],
            ep=target,
        )

    loop(ep_count - 1, lambda turn: rank_copy(ep_at(turn), me).start())
    loop(chips - 1, lambda turn: chip_copy(chip_at(turn)).start())
    block_copy(normed_ref, me).start()
    picks[me] = rank_ref[me]
    for one in loads:
        one.wait()

    for pair in range(pairs):

        @pl.when(chip < last)
        def _():
            up_copy(me, pair).start()

        @pl.when(core == 0)
        def _():
            side_copy(me, pair).start()

        if guests:

            @pl.when(chip == last)
            def _():
                guest_query(pair).start()

    units = [(member, index) for member in range(group) for index in range(tiles)]
    lane = lax.broadcasted_iota(jnp.int32, (rows, LANES), 1)
    scale = jnp.asarray(HEAD**-0.5, jnp.bfloat16)

    def attend(pair, slot, queries, sums, maxima, first):
        def score_unit(unit, way):
            member, index = unit
            span = (index + 1) * tile if first else rows
            query = queries[index * tile : (index + 1) * tile, lanes_at(pair, LANES)] * scale
            query = jnp.where(lane[:tile] // HEAD == member, query, jnp.zeros_like(query))
            gates = gate_ref[pair * group + member, :, lanes_at(slot, rows)]
            result = lax.dot_general(
                query,
                held[slot, pair, 0, :span, :],
                (((1,), (1,)), ((), ())),
                preferred_element_type=jnp.float32,
            )
            result = result - gates[:, :span]
            if first:
                q_pos = index * tile + lax.broadcasted_iota(jnp.int32, result.shape, 0)
                k_pos = lax.broadcasted_iota(jnp.int32, result.shape, 1)
                result = jnp.where(k_pos <= q_pos, result, neg_fill)
            scores[way][:, :span] = result
            top = jnp.max(result, axis=1, keepdims=True)
            tops[way][...] = jnp.broadcast_to(top, (tile, LANES))

        def value_unit(unit, way):
            member, index = unit
            head = pair * group + member
            q_rows = slice(index * tile, (index + 1) * tile)
            span = (index + 1) * tile if first else rows
            new_max = tops[way][...]
            if not first:
                old_max = maxima[head, q_rows, :]
                new_max = jnp.maximum(old_max, new_max)
            wide = jnp.concatenate([new_max] * (span // LANES), axis=1)
            probs = jnp.exp(scores[way][:, :span] - wide).astype(jnp.bfloat16)
            values = held[slot, pair, 1, :span, :]
            values = jnp.where(lane[:span] // HEAD == member, values, jnp.ones_like(values))
            add = jnp.dot(probs, values, preferred_element_type=jnp.float32)
            if not first:
                add = add + sums[head, q_rows, :] * jnp.exp(old_max - new_max)
            sums[head, q_rows, :] = add
            maxima[head, q_rows, :] = new_max

        score_unit(units[0], 0)
        for turn, unit in enumerate(units):
            if turn + 1 < len(units):
                score_unit(units[turn + 1], (turn + 1) % 2)
            value_unit(unit, turn % 2)

    def spread_pieces(turn):
        slot = chip_at(turn) * CORES + core
        plane_copy(slot, tp_me, tp_me).wait_recv()
        loop(tp_count - 1, lambda way: plane_copy(slot, tp_me, tp_at(way)).start())

    def share_blocks(turn):
        slot = chip_at(turn) * CORES + core
        loop(tp_count - 1, lambda way: plane_copy(slot, tp_at(way), tp_me).wait_recv())
        block_copy(tokens.at[slot], slot).start()

    def shared_stage():
        for one in weights[:2]:
            one.wait()
        both = jnp.dot(normed_ref[...], shared_both[...], preferred_element_type=jnp.float32)
        shared_all[tp_me] = silu_mul(both)
        loop(tp_count - 1, lambda way: shared_copy(tp_me, tp_at(way)).start())

    token_count = normed_ref.shape[0]
    slot_rows = arrived.shape[1]
    tail_rows = slot_rows - experts * main
    tail_at = experts * main

    def gather_block(slot, block):
        ranks = picks[slot].astype(jnp.float32)
        parts = []
        if main:
            order = lax.broadcasted_iota(jnp.int32, (main, token_count), 0).astype(jnp.float32)
            for expert in range(experts):
                hit = ranks[expert : expert + 1, :] == order
                parts.append(jnp.where(hit, 1.0, 0.0))
        if tail_rows:
            order = lax.broadcasted_iota(jnp.int32, (tail_rows, token_count), 0)
            found = jnp.zeros((tail_rows, token_count), jnp.float32)
            for expert in range(experts):
                begin = expert * tail
                wanted = (order - begin + main).astype(jnp.float32)
                hit = ranks[expert : expert + 1, :] == wanted
                inside = jnp.logical_and(order >= begin, order < begin + tail)
                found = jnp.where(jnp.logical_and(hit, inside), 1.0, found)
            parts.append(found)
        pick = jnp.concatenate(parts, axis=0).astype(jnp.bfloat16)
        rows_in = jnp.dot(pick, block, preferred_element_type=jnp.float32)
        arrived[slot] = rows_in.astype(jnp.bfloat16)

    def tail_select(value_of, width):
        order = lax.broadcasted_iota(jnp.int32, (ep_slots, tail_rows, width), 1)
        order = order.reshape(ep_slots * tail_rows, width)
        total = value_of(0)
        for expert in range(1, experts):
            total = jnp.where(order >= expert * tail, value_of(expert), total)
        return total

    def up_stage():
        own_block = pltpu.make_async_copy(normed_ref, tokens.at[me], stage_sem.at[0])
        own_block.start()

        def finish_blocks(index):
            slot = index * CORES + other
            block_copy(tokens.at[slot], slot).wait_recv()

        def finish_ranks(turn):
            rank_copy(ep_at(turn), ep_at(turn)).wait_recv()

        own_block.wait()
        loop(ep_count - 1, finish_ranks)
        loop(chips, finish_blocks)

        def gather(slot):
            if staged is None:
                gather_block(slot, tokens[slot])
            else:
                fetch = pltpu.make_async_copy(tokens.at[slot], staged, stage_sem.at[1])
                fetch.start()
                fetch.wait()
                gather_block(slot, staged[...])

        loop(ep_count, gather)
        for one in weights[2:4]:
            one.wait()
        depth = arrived.shape[2]
        if main:

            def expert_step(expert):
                span = pl.ds(pl.multiple_of(expert * main, main), main)
                block = arrived[:, span, :].reshape(ep_slots * main, depth)
                both = jnp.dot(block, gate_up[expert], preferred_element_type=jnp.float32)
                hidden[tp_me, :, span, :] = silu_mul(both).reshape(ep_slots, main, LANES)

            loop(experts, expert_step)
        if tail_rows:
            block = arrived[:, tail_at:, :].reshape(ep_slots * tail_rows, depth)
            both = tail_select(
                lambda e: jnp.dot(block, gate_up[e], preferred_element_type=jnp.float32),
                2 * LANES,
            )
            hidden[tp_me, :, tail_at:, :] = silu_mul(both).reshape(ep_slots, tail_rows, LANES)
        loop(tp_count - 1, lambda way: hidden_copy(tp_me, tp_at(way)).start())

    def down_stage():
        weights[4].wait()
        loop(tp_count - 1, lambda way: hidden_copy(tp_at(way), tp_at(way)).wait_recv())
        width = down.shape[2]

        def joined(span, count):
            parts = [
                hidden[piece, :, span, :].reshape(ep_slots * count, LANES)
                for piece in range(tp_count)
            ]
            return jnp.concatenate(parts, axis=1)

        if main:

            def expert_step(expert):
                span = pl.ds(pl.multiple_of(expert * main, main), main)
                out = jnp.dot(joined(span, main), down[expert], preferred_element_type=jnp.float32)
                results[:, span, :] = out.astype(jnp.bfloat16).reshape(ep_slots, main, width)

            loop(experts, expert_step)
        if tail_rows:
            block = joined(pl.ds(tail_at, tail_rows), tail_rows)
            out = tail_select(
                lambda e: jnp.dot(block, down[e], preferred_element_type=jnp.float32), width
            )
            out = out.astype(jnp.bfloat16).reshape(ep_slots, tail_rows, width)
            results[:, tail_at:, :] = out
        loop(ep_count - 1, lambda turn: result_copy(ep_at(turn), me).start())
        returned[me] = results[me]

    def ratio(sums, head):
        whole = sums[head]
        return whole / pltpu.roll(whole, HEAD, 1)

    def pair_out(sums, pair):
        joined = ratio(sums, pair * group)
        if group > 1:
            joined = jnp.where(lane < HEAD, joined, ratio(sums, pair * group + 1))
        return joined.astype(jnp.bfloat16)

    def send_guest(pair):
        guest_out[pair] = pair_out(guest_acc, pair)
        stats = jnp.zeros((rows, LANES), jnp.float32)
        for member in range(group):
            whole = guest_acc[pair * group + member]
            total = jnp.where(lane // HEAD == member, pltpu.roll(whole, HEAD, 1), whole)
            value = guest_max[pair * group + member] + jnp.log(total)
            stats = jnp.where(lane == member, value, stats)
        guest_lse[pair] = stats.T[:8, :]
        guest_result(pair).start()
        guest_stats(pair).start()

    def merge_guest(pair):
        guest_result(pair).wait_recv()
        guest_stats(pair).wait_recv()
        stats = jnp.concatenate([lse_in[pair]] * (LANES // 8), axis=0).T
        outer = guest_in[pair].astype(jnp.float32)
        for member in range(group):
            head = pair * group + member
            value = jnp.broadcast_to(stats[:, member : member + 1], (rows, LANES))
            new_max = jnp.maximum(row_max[head], value)
            part = jnp.where(lane // HEAD == member, outer, 1.0)
            acc[head] = acc[head] * jnp.exp(row_max[head] - new_max) + part * jnp.exp(
                value - new_max
            )

    def finish_pair(pair):
        if guests:

            @pl.when(chip == last)
            def _():
                merge_guest(pair)

        if wide_heads:
            heads_all[:, lanes_at(tp_me * pairs + pair, LANES)] = pair_out(acc, pair)
        else:
            heads_all[tp_me] = pair_out(acc, pair)
        loop(tp_count - 1, lambda way: heads_copy(tp_me, pair, tp_at(way)).start())

    reach = 1 if guests else chips
    deepest = jnp.where(chip == last, jnp.minimum(chip, reach), chip)
    step_count = deepest * CORES + core
    turns = 1 + max(CORES * (host if guests else last) + 1, CORES + 1)
    delay = 3 if guests else 0
    total = pairs * turns

    def remote_step(pair, step):
        turn = step - core + CORES
        own_core = turn % CORES == 0
        back = turn // CORES
        slot = (chip - back) * CORES + jnp.where(own_core, core, other)
        side_copy(slot, pair).wait_recv()

        @pl.when(jnp.logical_and(own_core, chip < (host if guests else last)))
        def _():
            up_copy(slot, pair).start()

        @pl.when(own_core)
        def _():
            side_copy(slot, pair).start()

        attend(pair, slot, q_own, acc, row_max, False)
        if guests:

            @pl.when(jnp.logical_and(chip == host, back >= 1))
            def _():
                @pl.when(step == core)
                def _():
                    guest_query(pair).wait_recv()
                    for member in range(group):
                        head = pair * group + member
                        guest_acc[head] = jnp.zeros((rows, LANES), jnp.float32)
                        guest_max[head] = jnp.full((rows, LANES), neg_fill, jnp.float32)

                attend(pair, slot, q_guest, guest_acc, guest_max, False)

    share_at = chips
    up_at = chips + 1
    down_at = total - 3

    def one_turn(index):
        pair = index // turns
        turn = index % turns

        @pl.when(jnp.logical_and(index >= 1, index < chips))
        def _():
            spread_pieces(index - 1)

        @pl.when(index == 1)
        def _():
            shared_stage()

        @pl.when(index == share_at)
        def _():
            loop(chips - 1, share_blocks)

        @pl.when(index == up_at)
        def _():
            up_stage()

        @pl.when(index == down_at)
        def _():
            down_stage()

        @pl.when(index < total)
        def _():
            @pl.when(turn == 0)
            def _():
                attend(pair, me, q_own, acc, row_max, True)

            @pl.when(jnp.logical_and(turn >= 1, turn <= step_count))
            def _():
                remote_step(pair, turn - 1)

            if guests:

                @pl.when(jnp.logical_and(chip == host, turn == turns - 1))
                def _():
                    send_guest(pair)

        late = index - jnp.where(chip == last, delay, 0)

        @pl.when(jnp.logical_and(late >= 0, late % turns == turns - 1))
        def _():
            @pl.when(late < total)
            def _():
                finish_pair(late // turns)

    loop(total + delay, one_turn)

    for pair in range(pairs):

        def finish_kv(back):
            slot = (chip - back) * CORES + core

            @pl.when(
                jnp.logical_or(
                    chip < (host if guests else last), jnp.logical_and(back == 0, chip < last)
                )
            )
            def _():
                up_copy(slot, pair).wait_send()

            @pl.when(back > 0)
            def _():
                side_copy(slot, pair).wait_send()

        loop(deepest + 1, finish_kv)

        @pl.when(core == 0)
        def _():
            side_copy(me, pair).wait_send()

        if guests:

            @pl.when(chip == last)
            def _():
                guest_query(pair).wait_send()

            @pl.when(chip == host)
            def _():
                guest_result(pair).wait_send()
                guest_stats(pair).wait_send()

    def finish_tokens(turn):
        target = chip_at(turn)
        slot = target * CORES + core
        chip_copy(target).wait_send()
        loop(tp_count - 1, lambda way: plane_copy(slot, tp_me, tp_at(way)).wait_send())
        block_copy(tokens.at[slot], slot).wait_send()

    loop(chips - 1, finish_tokens)
    block_copy(normed_ref, me).wait_send()

    def finish_peers(turn):
        rank_copy(ep_at(turn), me).wait_send()
        result_copy(ep_at(turn), me).wait_send()
        result_copy(ep_at(turn), ep_at(turn)).wait_recv()

    loop(ep_count - 1, finish_peers)

    def finish_plane(way):
        peer = tp_at(way)
        shared_copy(tp_me, peer).wait_send()
        shared_copy(peer, peer).wait_recv()
        hidden_copy(tp_me, peer).wait_send()
        for pair in range(pairs):
            heads_copy(tp_me, pair, peer).wait_send()
            heads_copy(peer, pair, peer).wait_recv()

    loop(tp_count - 1, finish_plane)


def slot_layout(capacity, experts):
    main = capacity // ROW_TILE * ROW_TILE
    tail = capacity - main
    tail_rows = -(-tail * experts // ROW_TILE) * ROW_TILE
    return main, tail, experts * main + tail_rows


def padded(a, axis, to):
    if a.shape[axis] == to:
        return a
    spare = [(0, 0)] * a.ndim
    spare[axis] = (0, to - a.shape[axis])
    return jnp.pad(a, spare)


def fused_block(
    query_rows,
    key_rows,
    value_rows,
    cum_gate,
    normed,
    ranks,
    capacity,
    expert_gate,
    expert_up,
    expert_down,
    shared_gate,
    shared_up,
):
    rows, width = query_rows.shape
    heads = width // HEAD
    pairs = (heads + 1) // 2
    ep_count = lax.axis_size("ep")
    tp_count = lax.axis_size("tp")
    chips = ep_count // CORES
    lanes = pairs * LANES
    tile = rows // 2 if rows % (2 * LANES) == 0 else rows
    query_rows, key_rows, value_rows = (
        padded(a, 1, lanes) for a in (query_rows, key_rows, value_rows)
    )
    experts, depth, span = expert_gate.shape
    columns = expert_down.shape[2]
    token_count = normed.shape[0]
    main, tail, slot_rows = slot_layout(capacity, experts)
    if span < LANES:
        expert_gate, expert_up = padded(expert_gate, 2, LANES), padded(expert_up, 2, LANES)
        shared_gate, shared_up = padded(shared_gate, 1, LANES), padded(shared_up, 1, LANES)
        expert_down = padded(expert_down.reshape(experts, tp_count, span, columns), 2, LANES)
        expert_down = expert_down.reshape(experts, tp_count * LANES, columns)
    inside = ep_count * token_count * depth * 2 <= 8 * 1024 * 1024
    bf16, f32 = jnp.bfloat16, jnp.float32
    vmem = pl.BlockSpec(memory_space=pltpu.VMEM)
    anywhere = pl.BlockSpec(memory_space=pl.ANY)
    heads_shape = (rows, tp_count * width) if width % LANES == 0 else (tp_count, rows, LANES)
    outs = [
        jax.ShapeDtypeStruct(heads_shape, bf16),
        jax.ShapeDtypeStruct((ep_count, slot_rows, columns), bf16),
        jax.ShapeDtypeStruct((tp_count, token_count, LANES), bf16),
    ]
    out_specs = [vmem] * 3
    token_shape = (ep_count, token_count, depth)
    scratch = []
    if inside:
        scratch.append(pltpu.VMEM(token_shape, bf16))
    else:
        outs.append(jax.ShapeDtypeStruct(token_shape, bf16))
        out_specs.append(anywhere)
    dma = pltpu.SemaphoreType.DMA
    scratch += [
        pltpu.VMEM((rows, lanes), bf16),
        pltpu.VMEM((rows, lanes), bf16),
        pltpu.VMEM((ep_count, pairs, 2, rows, LANES), bf16),
        pltpu.VMEM((heads, rows, LANES), f32),
        pltpu.VMEM((heads, rows, LANES), f32),
        pltpu.VMEM((heads, rows, LANES), f32),
        pltpu.VMEM((heads, rows, LANES), f32),
        pltpu.VMEM((pairs, rows, LANES), bf16),
        pltpu.VMEM((pairs, rows, LANES), bf16),
        pltpu.VMEM((pairs, 8, rows), f32),
        pltpu.VMEM((pairs, 8, rows), f32),
        pltpu.VMEM((tile, rows), f32),
        pltpu.VMEM((tile, rows), f32),
        pltpu.VMEM((tile, LANES), f32),
        pltpu.VMEM((tile, LANES), f32),
        pltpu.VMEM(ranks.shape, bf16),
    ]
    if not inside:
        scratch.append(pltpu.VMEM((token_count, depth), bf16))
    scratch += [
        pltpu.VMEM((ep_count, slot_rows, depth), bf16),
        pltpu.VMEM((experts, depth, 2 * LANES), bf16),
        pltpu.VMEM(expert_down.shape, bf16),
        pltpu.VMEM((depth, 2 * LANES), bf16),
        pltpu.VMEM((tp_count, ep_count, slot_rows, LANES), bf16),
        pltpu.VMEM((ep_count, slot_rows, columns), bf16),
        dma((6 + 2 * pairs,)),
        dma((ep_count, pairs)),
        dma((ep_count, pairs)),
        dma((ep_count, pairs)),
        dma((3, pairs)),
        dma((3, pairs)),
        dma((chips,)),
        dma((ep_count, tp_count)),
        dma((ep_count, tp_count)),
        dma((ep_count,)),
        dma((ep_count,)),
        dma((ep_count,)),
        dma((ep_count,)),
        dma((tp_count,)),
        dma((tp_count,)),
        dma((tp_count,)),
        dma((tp_count,)),
        dma((pairs, tp_count)),
        dma((pairs, tp_count)),
        dma((ep_count,)),
        dma((ep_count,)),
        dma((2,)),
    ]
    body = functools.partial(block_kernel, heads, main, tail)
    inputs = 11

    def kernel(*refs):
        refs = list(refs)
        if inside:
            refs.insert(inputs + 3 + 17, None)
        body(*refs)

    blocks = ep_count * rows * rows * heads
    results = pl.pallas_call(
        kernel,
        out_shape=outs,
        in_specs=[anywhere] * 3 + [vmem] * 3 + [anywhere] * 5,
        out_specs=out_specs,
        scratch_shapes=scratch,
        compiler_params=pltpu.CompilerParams(
            collective_id=0, has_side_effects=True, vmem_limit_bytes=58 * 1024 * 1024
        ),
        cost_estimate=pl.CostEstimate(
            flops=blocks * 2 * 512, bytes_accessed=8 * 1024 * 1024, transcendentals=blocks
        ),
        name="fused_block",
    )(
        query_rows,
        key_rows,
        value_rows,
        cum_gate[:, None, :],
        normed,
        ranks,
        expert_gate,
        expert_up,
        expert_down,
        shared_gate,
        shared_up,
    )
    heads_all, returned, shared_all = results[:3]
    if heads_all.ndim == 3:
        heads_all = heads_all[:, :, :width].transpose(1, 0, 2).reshape(rows, -1)
    shared_all = shared_all[:, :, :span].transpose(1, 0, 2).reshape(token_count, -1)
    return heads_all, returned, shared_all


def local(
    query_rows,
    key_rows,
    value_rows,
    cum_gate,
    out_weight,
    moe_input,
    moe_gain,
    routes,
    route_weight,
    expert_gate,
    expert_up,
    expert_down,
    shared_gate,
    shared_up,
    shared_down,
):
    token_count = moe_input.shape[0]
    top_count = routes.shape[1]
    local_experts = expert_gate.shape[0]
    ep_count = lax.axis_size("ep")
    expert_count = local_experts * ep_count
    capacity = 2 * token_count * top_count // expert_count
    moe_rows = moe_input.astype(jnp.float32)
    normed = (
        moe_rows
        * lax.rsqrt(jnp.mean(moe_rows * moe_rows, axis=1, keepdims=True) + norm_eps)
        * moe_gain
    ).astype(jnp.bfloat16)
    expert_ids = jnp.arange(expert_count, dtype=jnp.int32)
    chosen = routes[:, :, None] == expert_ids[None, None, :]
    named = jnp.any(chosen, axis=1)
    order = jnp.arange(token_count)
    earlier = (order[None, :] < order[:, None]).astype(jnp.bfloat16)
    ranks = jnp.dot(earlier, named.astype(jnp.bfloat16), preferred_element_type=jnp.float32)
    ranks = jnp.where(named, ranks.astype(jnp.int32), -1)
    rank_rows = ranks.astype(jnp.bfloat16).T.reshape(ep_count, local_experts, token_count)
    heads_all, returned, shared_all = fused_block(
        query_rows,
        key_rows,
        value_rows,
        cum_gate,
        normed,
        rank_rows,
        capacity,
        expert_gate,
        expert_up,
        expert_down,
        shared_gate,
        shared_up,
    )
    main, tail, slot_rows = slot_layout(capacity, local_experts)
    taken = jnp.sum(jnp.where(chosen, ranks[:, None, :], 0), axis=2)
    local_id = routes % local_experts
    spot = jnp.where(
        taken < main,
        local_id * main + taken,
        local_experts * main + local_id * tail + taken - main,
    )
    spot = spot + routes // local_experts * slot_rows
    spots = jnp.arange(ep_count * slot_rows, dtype=jnp.int32)
    weight = jnp.zeros((token_count, ep_count * slot_rows), jnp.float32)
    for choice in range(top_count):
        hit = spot[:, choice : choice + 1] == spots[None, :]
        weight = jnp.where(hit, route_weight[:, choice : choice + 1], weight)
    weight_high = lax.reduce_precision(weight, 8, 7)
    weight_low = weight - weight_high
    results = returned.reshape(ep_count * slot_rows, -1)
    moe_total = jnp.dot(shared_all, shared_down, preferred_element_type=jnp.float32)
    for part in (weight_high, weight_low):
        moe_total = moe_total + jnp.dot(
            part.astype(jnp.bfloat16), results, preferred_element_type=jnp.float32
        )
    mixer_sum = jnp.dot(heads_all, out_weight, preferred_element_type=jnp.float32)
    return (mixer_sum.astype(jnp.bfloat16), moe_total.astype(jnp.bfloat16))


def solution(mesh):
    placed = (
        P("ep", "tp"),
        P("ep", "tp"),
        P("ep", "tp"),
        P("tp", None),
        P(None, "tp"),
        P("ep", None),
        P(),
        P("ep", None),
        P("ep", None),
        P("ep", None, "tp"),
        P("ep", None, "tp"),
        P("ep", None, "tp"),
        P(None, "tp"),
        P(None, "tp"),
        P(None, "tp"),
    )
    return jax.shard_map(
        local, mesh=mesh, in_specs=placed, out_specs=(P("ep", "tp"), P("ep", "tp")), check_vma=False
    )
```

time: 184 us -> 133 us (0.72); the launches traced: 182 us -> 133 us
  matrix products: 21.8 us -> 5.72 us
  Pallas kernels: 131 us -> 118 us
  local copies, waits for them, and re-layouts: 14.8 us -> 3.05 us
  starting transfers between devices: 5.4 us -> 0 us
    dot_general x9 -> x2, matrix products: 17.2 us -> 1.9 us  [local(): jnp.dot(part.astype(jnp.bfloat16), results, preferred_element_type=jnp.fl...]
    pallas_call x3 -> x1, Pallas kernels: 131 us -> 118 us  [fused_block(): pl.pallas_call(kernel, out_shape=outs, in_specs=[anywhere] * 3 + [vmem] *...]
    convert_element_type x5 -> x0, local copies, waits for them, and re-layouts: 8.82 us -> none  [the longest x2 4.24 us: local(): spread = jnp.where(place, weight[:, :, None], 0.0).astype(jnp.bfloat16)]
    all_to_all x1 -> x0, starting transfers between devices: 5.4 us -> none  [local(): lax.all_to_all(result, 'ep', split_axis=0, concat_axis=0, tiled=True)]
    reshape x2 -> x0, local copies, waits for them, and re-layouts: 2.92 us -> none  [the longest x1 2.15 us: local(): returned = returned.reshape(expert_count * capacity, column_count)]
  transfers between devices with their start and end apart: 1 -> 0, of which waited for: 0 -> 0; matrix products, arithmetic and copies ran while one was open for 5% -> 0% of each run, Pallas kernels for 12% -> 0%
where the time goes in v2:
time: 133 us
  Pallas kernels  118 us (89%)
  matrix products  5.72 us (4%)
  other arithmetic  5.48 us (4%)
  local copies, waits for them, and re-layouts  3.05 us (2%)
    pallas_call x1, Pallas kernels, fused_block(): pl.pallas_call(kernel, out_shape=outs, in_specs=[anywhere] * 3 + [vmem] *...  118 us
    dot_general x1, matrix products, local(): jnp.dot(heads_all, out_weight, preferred_element_type=jnp.float32)  3.4 us

profile of v2, /device:TPU:25, one launch (start us, length us, event | category | flops | bytes accessed | tf_op | source)
XLA Modules:
  0.0 132.7 jit_solution(16220223105843182191)
XLA Ops:
  0.6 0.0 copy-start
  0.6 0.0 copy-start.1
  0.7 1.5 %fusion = f32[192]{0:T(256)S(1)} fusion(bf16[192,2048]{1,0:T(8,128)(2,1)} %param.20), kind=kLoop, calls=%fused_computation.2 | loop fusion | flops 1179456 | bytes 787200 | tf_op jit(solution)/shard_map/reduce_sum | solution.py:856
  2.2 0.8 fusion.32
  3.0 0.7 fusion.24
  3.7 0.2 fusion.4
  3.8 0.7 select_reduce_fusion
  4.6 0.6 reshape.24.refs_5_
  5.2 0.7 fusion.26
  5.9 1.6 %broadcast_in_dim.56.refs_3_ = f32[4,1,6144]{2,1,0:T(1,128)} reshape(f32[4,6144]{1,0:T(4,128)} %param.18) | data formatting | bytes 196608 | tf_op jit(solution)/shard_map/broadcast_in_dim | solution.py:814
  7.5 0.0 copy-done.1
  7.5 1.8 %fusion.2.refs_4_ = bf16[192,2048]{1,0:T(8,128)(2,1)} fusion(bf16[192,2048]{1,0:T(8,128)(2,1)S(1)} %copy-done.1, f32[2048]{0:T(1024)} %param.21, f32[192]{0:T(256)S(1)} %add_rsqrt_fusion), kind=kLoop, calls=%fused_computation.4 | loop fusion | flops 1572864 | bytes 1581824 | tf_op jit(solution)/shard_map/convert_element_type | solution.py:858
  9.3 117.7 %fused_block.1 = (bf16[768,1024]{1,0:T(8,128)(2,1)}, bf16[8,144,512]{2,1,0:T(8,128)(2,1)}, bf16[4,192,128]{2,1,0:T(8,128)(2,1)}) custom-call(bf16[768,256]{1,0:T(8,128)(2,1)} %refs_0_.1, bf16[768,256]{1,0:T(8,128)(2,1)} %refs_1_.1, bf16[768,256]{1,0:T(8,128)(2,1)} %refs_2_.1, f32[4,1,6144]{2,1,0:T(1,128)} %broadcast_in_dim.56.refs_3_, ...), custom_call_target="tpu_custom_call" | custom-call | flops 19327352832 | bytes 8388608 | tf_op jit(solution)/shard_map/fused_block/pallas_call | solution.py:797
  127.0 0.0 copy-done
  127.0 0.0 copy-start.2
  127.1 0.0 copy-start.3
  127.1 0.0 copy-start.4
  127.1 3.4 %convolution_convert_fusion = bf16[768,512]{1,0:T(8,128)(2,1)} fusion(bf16[768,1024]{1,0:T(8,128)(2,1)} %get-tuple-element.5, bf16[1024,512]{1,0:T(8,128)(2,1)S(1)} %copy-done), kind=kOutput, calls=%fused_computation.5 | convolution fusion | flops 805699584 | bytes 3407872 | tf_op jit(solution)/shard_map/dot_general | solution.py:903
  130.5 0.0 copy-done.2
  130.5 0.0 copy-done.3
  130.5 0.3 fusion.21
  130.7 0.0 copy-done.4
  130.8 0.6 convolution_add_fusion.1
  131.4 1.3 fusion.3
  (3 shorter events, 0.0 us)
Async XLA Ops:
  0.6 126.4 %copy-start = (bf16[1024,512]{1,0:T(8,128)(2,1)S(1)}, bf16[1024,512]{1,0:T(8,128)(2,1)}, u32[]{:S(2)}) copy-start(bf16[1024,512]{1,0:T(8,128)(2,1)} %param.19) | copy-start | bytes 3145732
  0.6 6.9 %copy-start.1 = (bf16[192,2048]{1,0:T(8,128)(2,1)S(1)}, bf16[192,2048]{1,0:T(8,128)(2,1)}, u32[]{:S(2)}) copy-start(bf16[192,2048]{1,0:T(8,128)(2,1)} %param.20) | copy-start | bytes 2359300
  127.0 3.4 %copy-start.2 = (bf16[512,512]{1,0:T(8,128)(2,1)S(1)}, bf16[512,512]{1,0:T(8,128)(2,1)}, u32[]{:S(2)}) copy-start(bf16[512,512]{1,0:T(8,128)(2,1)} %param.29) | copy-start | bytes 1572868
  127.1 3.4 %copy-start.3 = (bf16[4,192,128]{2,1,0:T(8,128)(2,1)S(1)}, bf16[4,192,128]{2,1,0:T(8,128)(2,1)}, u32[]{:S(2)}) copy-start(bf16[4,192,128]{2,1,0:T(8,128)(2,1)} %get-tuple-element.6) | copy-start | bytes 589828
  127.1 3.7 %copy-start.4 = (bf16[8,144,512]{2,1,0:T(8,128)(2,1)S(1)}, bf16[8,144,512]{2,1,0:T(8,128)(2,1)}, u32[]{:S(2)}) copy-start(bf16[8,144,512]{2,1,0:T(8,128)(2,1)} %get-tuple-element.7) | copy-start | bytes 3538948

commit v3 on v2

--- a/solution.py
+++ b/solution.py
@@ -29,17 +29,30 @@
     k_hbm,
     v_hbm,
     gate_ref,
-    normed_ref,
-    rank_ref,
+    routes_ref,
+    weight_ref,
+    gain_ref,
+    moe_hbm,
     expert_gate,
     expert_up,
     expert_down,
     shared_gate,
     shared_up,
+    shared_down,
+    out_weight,
+    mixer_out,
+    moe_out,
+    tokens,
+    moe_rows,
+    normed_ref,
+    rank_ref,
     heads_all,
     returned,
     shared_all,
-    tokens,
+    spread_high,
+    spread_low,
+    mix_weight,
+    shared_last,
     q_own,
     q_guest,
     held,
@@ -61,7 +74,8 @@
     gate_up,
     down,
     shared_both,
-    hidden,
+    hidden_main,
+    hidden_tail,
     results,
     load_sem,
     up_send,
@@ -72,6 +86,7 @@
     chip_send,
     plane_send,
     piece_recv,
+    half_recv,
     block_send,
     block_recv,
     rank_send,
@@ -87,6 +102,7 @@
     stage_sem,
 ):
     ep_slots, pairs, _, rows, _ = held.shape
+    tp_slots = shared_all.shape[0]
     group = min(2, heads)
     experts = expert_gate.shape[0]
     tile = tops_even.shape[0]
@@ -118,7 +134,11 @@
         pl.semaphore_signal(barrier, inc=1, device_id=where)
 
     def chip_at(turn):
-        return lax.rem(chip + turn + 1, chips)
+        found, way, bit = 0, turn + 1, 1
+        while bit < chips:
+            found = found + ((chip // bit) % 2 + (way // bit) % 2) % 2 * bit
+            bit *= 2
+        return found
 
     def tp_at(turn):
         return lax.rem(tp_me + turn + 1, tp_count)
@@ -130,7 +150,8 @@
         return pl.ds(pl.multiple_of(index * width, width), width)
 
     loads = [
-        pltpu.make_async_copy(q_hbm, q_own, load_sem.at[0]),
+        pltpu.make_async_copy(moe_hbm, moe_rows, load_sem.at[0]),
+        pltpu.make_async_copy(q_hbm, q_own, load_sem.at[1]),
     ]
     for pair in range(pairs):
         lanes = pl.ds(pair * LANES, LANES)
@@ -149,6 +170,8 @@
         (expert_gate, gate_up.at[:, :, pl.ds(0, LANES)]),
         (expert_up, gate_up.at[:, :, pl.ds(LANES, LANES)]),
         (expert_down, down),
+        (shared_down, shared_last),
+        (out_weight, mix_weight),
     ):
         index = len(loads) + len(weights)
         weights.append(pltpu.make_async_copy(source, place, load_sem.at[index]))
@@ -157,6 +180,77 @@
 
     loop(ep_count - 1, lambda turn: greet(ep=ep_at(turn)))
     loop(tp_count - 1, lambda turn: greet(tp=tp_at(turn)))
+
+    token_count = normed_ref.shape[0]
+    slot_rows = arrived.shape[1]
+    tail_rows = slot_rows - experts * main
+    tail_at = experts * main
+    loads[0].wait()
+    token = moe_rows[...].astype(jnp.float32)
+    square = jnp.mean(token * token, axis=1, keepdims=True)
+    token = token * lax.rsqrt(square + norm_eps) * gain_ref[...]
+    normed_ref[...] = token.astype(jnp.bfloat16)
+
+    expert_lanes = -(-experts * ep_slots // LANES) * LANES
+    top_count = routes_ref.shape[0]
+    turned_shape = (expert_lanes, token_count)
+    expert_id = lax.broadcasted_iota(jnp.int32, turned_shape, 0)
+    named = expert_id == routes_ref[0:1, :]
+    for choice in range(1, top_count):
+        named = jnp.logical_or(named, expert_id == routes_ref[choice : choice + 1, :])
+    named = jnp.where(named, 1.0, 0.0)
+    square_shape = (token_count, token_count)
+    first_id = lax.broadcasted_iota(jnp.int32, square_shape, 0)
+    second_id = lax.broadcasted_iota(jnp.int32, square_shape, 1)
+    earlier = jnp.where(first_id < second_id, 1.0, 0.0).astype(jnp.bfloat16)
+    turned = jnp.dot(named.astype(jnp.bfloat16), earlier, preferred_element_type=jnp.float32)
+    turned = jnp.where(named > 0.0, turned, -1.0)
+    for owner in range(ep_slots):
+        rank_ref[owner] = turned[owner * experts : (owner + 1) * experts, :]
+
+    def spread_stage():
+        owner = jnp.zeros(turned_shape, jnp.int32)
+        for index in range(1, ep_slots):
+            owner = owner + jnp.where(expert_id >= index * experts, 1, 0)
+        local_id = (expert_id - owner * experts).astype(jnp.float32)
+        spot = jnp.where(
+            turned < main,
+            local_id * main + turned,
+            local_id * tail + turned + (tail_at - main),
+        )
+        order = lax.broadcasted_iota(jnp.int32, (ROW_TILE, token_count), 0)
+        table = jnp.zeros((ROW_TILE, token_count), jnp.float32)
+        for choice in range(top_count):
+            hit = expert_id == routes_ref[choice : choice + 1, :]
+            place = jnp.sum(jnp.where(hit, spot, 0.0), axis=0, keepdims=True)
+            home = jnp.sum(jnp.where(hit, owner, 0).astype(jnp.float32), axis=0, keepdims=True)
+            weight = weight_ref[choice : choice + 1, :]
+            high = weight.astype(jnp.bfloat16).astype(jnp.float32)
+            for part, value in enumerate((place, home, high, weight - high)):
+                table = jnp.where(order == part * top_count + choice, value, table)
+        same = jnp.where(first_id == second_id, 1.0, 0.0).astype(jnp.bfloat16)
+        table = lax.dot_general(
+            same,
+            table.astype(jnp.bfloat16),
+            (((1,), (1,)), ((), ())),
+            preferred_element_type=jnp.float32,
+        )
+        width = ep_slots * slot_rows
+        spots = lax.broadcasted_iota(jnp.int32, (token_count, width), 1).astype(jnp.float32)
+        high = jnp.zeros((token_count, width), jnp.float32)
+        low = jnp.zeros((token_count, width), jnp.float32)
+
+        def column(part, choice):
+            index = part * top_count + choice
+            return table[:, index : index + 1]
+
+        for choice in range(top_count):
+            hit = spots == column(0, choice) + column(1, choice) * slot_rows
+            high = jnp.where(hit, column(2, choice), high)
+            low = jnp.where(hit, column(3, choice), low)
+        spread_high[...] = high.astype(jnp.bfloat16)
+        spread_low[...] = low.astype(jnp.bfloat16)
+
     pl.semaphore_wait(barrier, ep_count + tp_count - 2)
 
     def remote(source, target, send, recv, **where):
@@ -222,6 +316,32 @@
             place, place, plane_send.at[slot, target], piece_recv.at[slot, piece], tp=target
         )
 
+    x_peer = tp_me + 1 - 2 * (tp_me % 2)
+    y_peer = tp_me + 2 - 4 * (tp_me // 2 % 2)
+    far_peer = x_peer + 2 - 4 * (x_peer // 2 % 2)
+    relay = tp_slots == 4 and normed_ref.shape[0] % (2 * ROW_TILE) == 0
+
+    def near_copy(slot, piece, way):
+        place = tokens.at[slot, :, lanes_at(piece, columns)]
+        return remote(
+            place,
+            place,
+            plane_send.at[slot, way],
+            piece_recv.at[slot, piece],
+            tp=(x_peer, y_peer)[way],
+        )
+
+    def half_copy(slot, piece, part):
+        half = normed_ref.shape[0] // 2
+        place = tokens.at[slot, pl.ds(part * half, half), lanes_at(piece, columns)]
+        return remote(
+            place,
+            place,
+            plane_send.at[slot, 2 + part],
+            half_recv.at[slot, part],
+            tp=(y_peer, x_peer)[part],
+        )
+
     def block_copy(source, slot):
         return remote(
             source,
@@ -235,9 +355,13 @@
         place = shared_all.at[owner]
         return remote(place, place, shared_send.at[target], shared_recv.at[owner], tp=target)
 
-    def hidden_copy(owner, target):
-        place = hidden.at[owner]
-        return remote(place, place, hidden_send.at[target], hidden_recv.at[owner], tp=target)
+    def hidden_copy(owner, part, target):
+        place = hidden_tail.at[owner]
+        if not (isinstance(part, int) and part == experts):
+            place = hidden_main.at[owner, part]
+        return remote(
+            place, place, hidden_send.at[part, target], hidden_recv.at[part, owner], tp=target
+        )
 
     wide_heads = heads * HEAD % LANES == 0
 
@@ -265,7 +389,7 @@
     loop(chips - 1, lambda turn: chip_copy(chip_at(turn)).start())
     block_copy(normed_ref, me).start()
     picks[me] = rank_ref[me]
-    for one in loads:
+    for one in loads[1:]:
         one.wait()
 
     for pair in range(pairs):
@@ -294,7 +418,7 @@
             span = (index + 1) * tile if first else rows
             query = queries[index * tile : (index + 1) * tile, lanes_at(pair, LANES)] * scale
             query = jnp.where(lane[:tile] // HEAD == member, query, jnp.zeros_like(query))
-            gates = gate_ref[pair * group + member, :, lanes_at(slot, rows)]
+            gates = gate_ref[pl.ds(pair * group + member, 1), lanes_at(slot, rows)]
             result = lax.dot_general(
                 query,
                 held[slot, pair, 0, :span, :],
@@ -338,12 +462,32 @@
     def spread_pieces(turn):
         slot = chip_at(turn) * CORES + core
         plane_copy(slot, tp_me, tp_me).wait_recv()
-        loop(tp_count - 1, lambda way: plane_copy(slot, tp_me, tp_at(way)).start())
+        if relay:
+            for way in range(2):
+                near_copy(slot, tp_me, way).start()
+        else:
+            loop(tp_count - 1, lambda way: plane_copy(slot, tp_me, tp_at(way)).start())
+
+    def relay_pieces(turn):
+        slot = chip_at(turn) * CORES + core
+        for way, peer in enumerate((x_peer, y_peer)):
+            near_copy(slot, peer, way).wait_recv()
+            half_copy(slot, peer, way).start()
+
+    def token_stage():
+        loop(chips - 1, spread_pieces)
+        if relay:
+            loop(chips - 1, relay_pieces)
 
     def share_blocks(turn):
         slot = chip_at(turn) * CORES + core
-        loop(tp_count - 1, lambda way: plane_copy(slot, tp_at(way), tp_me).wait_recv())
+        if relay:
+            for part in range(2):
+                half_copy(slot, far_peer, part).wait_recv()
+        else:
+            loop(tp_count - 1, lambda way: plane_copy(slot, tp_at(way), tp_me).wait_recv())
         block_copy(tokens.at[slot], slot).start()
+        gather(slot)
 
     def shared_stage():
         for one in weights[:2]:
@@ -352,13 +496,8 @@
         shared_all[tp_me] = silu_mul(both)
         loop(tp_count - 1, lambda way: shared_copy(tp_me, tp_at(way)).start())
 
-    token_count = normed_ref.shape[0]
-    slot_rows = arrived.shape[1]
-    tail_rows = slot_rows - experts * main
-    tail_at = experts * main
-
     def gather_block(slot, block):
-        ranks = picks[slot].astype(jnp.float32)
+        ranks = picks[slot]
         parts = []
         if main:
             order = lax.broadcasted_iota(jnp.int32, (main, token_count), 0).astype(jnp.float32)
@@ -387,79 +526,76 @@
             total = jnp.where(order >= expert * tail, value_of(expert), total)
         return total
 
+    def gather(slot):
+        if staged is None:
+            gather_block(slot, tokens[slot])
+        else:
+            fetch = pltpu.make_async_copy(tokens.at[slot], staged, stage_sem.at[0])
+            fetch.start()
+            fetch.wait()
+            gather_block(slot, staged[...])
+
+    def share_stage():
+        loop(ep_count - 1, lambda turn: rank_copy(ep_at(turn), ep_at(turn)).wait_recv())
+        gather_block(me, normed_ref[...])
+        loop(chips - 1, share_blocks)
+
     def up_stage():
-        own_block = pltpu.make_async_copy(normed_ref, tokens.at[me], stage_sem.at[0])
-        own_block.start()
-
-        def finish_blocks(index):
+        def finish_block(index):
             slot = index * CORES + other
             block_copy(tokens.at[slot], slot).wait_recv()
-
-        def finish_ranks(turn):
-            rank_copy(ep_at(turn), ep_at(turn)).wait_recv()
-
-        own_block.wait()
-        loop(ep_count - 1, finish_ranks)
-        loop(chips, finish_blocks)
-
-        def gather(slot):
-            if staged is None:
-                gather_block(slot, tokens[slot])
-            else:
-                fetch = pltpu.make_async_copy(tokens.at[slot], staged, stage_sem.at[1])
-                fetch.start()
-                fetch.wait()
-                gather_block(slot, staged[...])
-
-        loop(ep_count, gather)
+            gather(slot)
+
+        finish_block(chip)
+        loop(chips - 1, lambda turn: finish_block(chip_at(turn)))
         for one in weights[2:4]:
             one.wait()
         depth = arrived.shape[2]
-        if main:
-
-            def expert_step(expert):
-                span = pl.ds(pl.multiple_of(expert * main, main), main)
-                block = arrived[:, span, :].reshape(ep_slots * main, depth)
-                both = jnp.dot(block, gate_up[expert], preferred_element_type=jnp.float32)
-                hidden[tp_me, :, span, :] = silu_mul(both).reshape(ep_slots, main, LANES)
-
-            loop(experts, expert_step)
         if tail_rows:
             block = arrived[:, tail_at:, :].reshape(ep_slots * tail_rows, depth)
             both = tail_select(
                 lambda e: jnp.dot(block, gate_up[e], preferred_element_type=jnp.float32),
                 2 * LANES,
             )
-            hidden[tp_me, :, tail_at:, :] = silu_mul(both).reshape(ep_slots, tail_rows, LANES)
-        loop(tp_count - 1, lambda way: hidden_copy(tp_me, tp_at(way)).start())
+            hidden_tail[tp_me] = silu_mul(both)
+            loop(tp_count - 1, lambda way: hidden_copy(tp_me, experts, tp_at(way)).start())
+        if main:
+
+            def expert_step(expert):
+                span = pl.ds(pl.multiple_of(expert * main, main), main)
+                block = arrived[:, span, :].reshape(ep_slots * main, depth)
+                both = jnp.dot(block, gate_up[expert], preferred_element_type=jnp.float32)
+                hidden_main[tp_me, expert] = silu_mul(both)
+                loop(tp_count - 1, lambda way: hidden_copy(tp_me, expert, tp_at(way)).start())
+
+            loop(experts, expert_step)
 
     def down_stage():
         weights[4].wait()
-        loop(tp_count - 1, lambda way: hidden_copy(tp_at(way), tp_at(way)).wait_recv())
         width = down.shape[2]
 
-        def joined(span, count):
-            parts = [
-                hidden[piece, :, span, :].reshape(ep_slots * count, LANES)
-                for piece in range(tp_count)
-            ]
-            return jnp.concatenate(parts, axis=1)
-
-        if main:
-
-            def expert_step(expert):
-                span = pl.ds(pl.multiple_of(expert * main, main), main)
-                out = jnp.dot(joined(span, main), down[expert], preferred_element_type=jnp.float32)
-                results[:, span, :] = out.astype(jnp.bfloat16).reshape(ep_slots, main, width)
-
-            loop(experts, expert_step)
+        def arrival(part):
+            loop(tp_count - 1, lambda way: hidden_copy(tp_at(way), part, tp_me).wait_recv())
+
         if tail_rows:
-            block = joined(pl.ds(tail_at, tail_rows), tail_rows)
+            arrival(experts)
+            block = jnp.concatenate([hidden_tail[piece] for piece in range(tp_slots)], axis=1)
             out = tail_select(
                 lambda e: jnp.dot(block, down[e], preferred_element_type=jnp.float32), width
             )
             out = out.astype(jnp.bfloat16).reshape(ep_slots, tail_rows, width)
             results[:, tail_at:, :] = out
+        if main:
+
+            def expert_step(expert):
+                arrival(expert)
+                span = pl.ds(pl.multiple_of(expert * main, main), main)
+                pieces = [hidden_main[piece, expert] for piece in range(tp_slots)]
+                block = jnp.concatenate(pieces, axis=1)
+                out = jnp.dot(block, down[expert], preferred_element_type=jnp.float32)
+                results[:, span, :] = out.astype(jnp.bfloat16).reshape(ep_slots, main, width)
+
+            loop(experts, expert_step)
         loop(ep_count - 1, lambda turn: result_copy(ep_at(turn), me).start())
         returned[me] = results[me]
 
@@ -469,7 +605,9 @@
 
     def pair_out(sums, pair):
         joined = ratio(sums, pair * group)
-        if group > 1:
+        if group == 1:
+            joined = jnp.where(lane < HEAD, joined, 0.0)
+        else:
             joined = jnp.where(lane < HEAD, joined, ratio(sums, pair * group + 1))
         return joined.astype(jnp.bfloat16)
 
@@ -515,9 +653,9 @@
     reach = 1 if guests else chips
     deepest = jnp.where(chip == last, jnp.minimum(chip, reach), chip)
     step_count = deepest * CORES + core
-    turns = 1 + max(CORES * (host if guests else last) + 1, CORES + 1)
-    delay = 3 if guests else 0
-    total = pairs * turns
+    steps = max(CORES * (host if guests else last) + 1, CORES + 1)
+    delay = 3 if guests else 1
+    total = pairs * (steps + 1)
 
     def remote_step(pair, step):
         turn = step - core + CORES
@@ -549,57 +687,45 @@
 
                 attend(pair, slot, q_guest, guest_acc, guest_max, False)
 
-    share_at = chips
-    up_at = chips + 1
-    down_at = total - 3
+    hooks = (
+        (1, shared_stage),
+        (1, spread_stage),
+        (pairs, token_stage),
+        (pairs + 1, share_stage),
+        (pairs + 2, up_stage),
+        (total, down_stage),
+    )
 
     def one_turn(index):
-        pair = index // turns
-        turn = index % turns
-
-        @pl.when(jnp.logical_and(index >= 1, index < chips))
+        for at, stage in hooks:
+            pl.when(index == at)(stage)
+
+        @pl.when(index < pairs)
         def _():
-            spread_pieces(index - 1)
-
-        @pl.when(index == 1)
+            attend(index, me, q_own, acc, row_max, True)
+
+        @pl.when(jnp.logical_and(index >= pairs, index < total))
         def _():
-            shared_stage()
-
-        @pl.when(index == share_at)
-        def _():
-            loop(chips - 1, share_blocks)
-
-        @pl.when(index == up_at)
-        def _():
-            up_stage()
-
-        @pl.when(index == down_at)
-        def _():
-            down_stage()
-
-        @pl.when(index < total)
-        def _():
-            @pl.when(turn == 0)
+            pair = (index - pairs) // steps
+            step = (index - pairs) % steps
+
+            @pl.when(step < step_count)
             def _():
-                attend(pair, me, q_own, acc, row_max, True)
-
-            @pl.when(jnp.logical_and(turn >= 1, turn <= step_count))
-            def _():
-                remote_step(pair, turn - 1)
+                remote_step(pair, step)
 
             if guests:
 
-                @pl.when(jnp.logical_and(chip == host, turn == turns - 1))
+                @pl.when(jnp.logical_and(chip == host, step == steps - 1))
                 def _():
                     send_guest(pair)
 
-        late = index - jnp.where(chip == last, delay, 0)
-
-        @pl.when(jnp.logical_and(late >= 0, late % turns == turns - 1))
+        late = index - pairs - jnp.where(chip == last, delay, 0)
+
+        @pl.when(jnp.logical_and(late >= 0, late < pairs * steps))
         def _():
-            @pl.when(late < total)
+            @pl.when(late % steps == steps - 1)
             def _():
-                finish_pair(late // turns)
+                finish_pair(late // steps)
 
     loop(total + delay, one_turn)
 
@@ -641,7 +767,12 @@
         target = chip_at(turn)
         slot = target * CORES + core
         chip_copy(target).wait_send()
-        loop(tp_count - 1, lambda way: plane_copy(slot, tp_me, tp_at(way)).wait_send())
+        if relay:
+            for way, peer in enumerate((x_peer, y_peer)):
+                near_copy(slot, tp_me, way).wait_send()
+                half_copy(slot, peer, way).wait_send()
+        else:
+            loop(tp_count - 1, lambda way: plane_copy(slot, tp_me, tp_at(way)).wait_send())
         block_copy(tokens.at[slot], slot).wait_send()
 
     loop(chips - 1, finish_tokens)
@@ -658,12 +789,28 @@
         peer = tp_at(way)
         shared_copy(tp_me, peer).wait_send()
         shared_copy(peer, peer).wait_recv()
-        hidden_copy(tp_me, peer).wait_send()
+        for part in range(experts + 1):
+            if tail_rows if part == experts else main:
+                hidden_copy(tp_me, part, peer).wait_send()
         for pair in range(pairs):
             heads_copy(tp_me, pair, peer).wait_send()
             heads_copy(peer, pair, peer).wait_recv()
 
     loop(tp_count - 1, finish_plane)
+    for one in weights[5:]:
+        one.wait()
+    shared_hidden = jnp.concatenate([shared_all[piece] for piece in range(tp_slots)], axis=1)
+    back = returned[...].reshape(ep_slots * slot_rows, returned.shape[2])
+    sums = jnp.dot(shared_hidden, shared_last[...], preferred_element_type=jnp.float32)
+    for part in (spread_high, spread_low):
+        sums = sums + jnp.dot(part[...], back, preferred_element_type=jnp.float32)
+    moe_out[...] = sums.astype(jnp.bfloat16)
+    if wide_heads:
+        mixed = heads_all[...]
+    else:
+        mixed = jnp.concatenate([heads_all[piece] for piece in range(tp_slots)], axis=1)
+    mixed = jnp.dot(mixed, mix_weight[...], preferred_element_type=jnp.float32)
+    mixer_out[...] = mixed.astype(jnp.bfloat16)
 
 
 def slot_layout(capacity, experts):
@@ -686,14 +833,17 @@
     key_rows,
     value_rows,
     cum_gate,
-    normed,
-    ranks,
-    capacity,
+    routes,
+    route_weight,
+    moe_gain,
+    moe_input,
     expert_gate,
     expert_up,
     expert_down,
     shared_gate,
     shared_up,
+    shared_down,
+    out_weight,
 ):
     rows, width = query_rows.shape
     heads = width // HEAD
@@ -708,24 +858,29 @@
     )
     experts, depth, span = expert_gate.shape
     columns = expert_down.shape[2]
-    token_count = normed.shape[0]
+    token_count = moe_input.shape[0]
+    capacity = 2 * token_count * routes.shape[1] // (experts * ep_count)
     main, tail, slot_rows = slot_layout(capacity, experts)
     if span < LANES:
         expert_gate, expert_up = padded(expert_gate, 2, LANES), padded(expert_up, 2, LANES)
         shared_gate, shared_up = padded(shared_gate, 1, LANES), padded(shared_up, 1, LANES)
         expert_down = padded(expert_down.reshape(experts, tp_count, span, columns), 2, LANES)
         expert_down = expert_down.reshape(experts, tp_count * LANES, columns)
+        shared_down = padded(shared_down.reshape(tp_count, span, columns), 1, LANES)
+        shared_down = shared_down.reshape(tp_count * LANES, columns)
     inside = ep_count * token_count * depth * 2 <= 8 * 1024 * 1024
     bf16, f32 = jnp.bfloat16, jnp.float32
     vmem = pl.BlockSpec(memory_space=pltpu.VMEM)
     anywhere = pl.BlockSpec(memory_space=pl.ANY)
+    if width % LANES:
+        out_weight = padded(out_weight.reshape(tp_count, width, columns), 1, LANES)
+        out_weight = out_weight.reshape(tp_count * LANES, columns)
     heads_shape = (rows, tp_count * width) if width % LANES == 0 else (tp_count, rows, LANES)
     outs = [
-        jax.ShapeDtypeStruct(heads_shape, bf16),
-        jax.ShapeDtypeStruct((ep_count, slot_rows, columns), bf16),
-        jax.ShapeDtypeStruct((tp_count, token_count, LANES), bf16),
+        jax.ShapeDtypeStruct((rows, columns), bf16),
+        jax.ShapeDtypeStruct((token_count, columns), bf16),
     ]
-    out_specs = [vmem] * 3
+    out_specs = [vmem] * 2
     token_shape = (ep_count, token_count, depth)
     scratch = []
     if inside:
@@ -735,6 +890,16 @@
         out_specs.append(anywhere)
     dma = pltpu.SemaphoreType.DMA
     scratch += [
+        pltpu.VMEM((token_count, depth), bf16),
+        pltpu.VMEM((token_count, depth), bf16),
+        pltpu.VMEM((ep_count, experts, token_count), f32),
+        pltpu.VMEM(heads_shape, bf16),
+        pltpu.VMEM((ep_count, slot_rows, columns), bf16),
+        pltpu.VMEM((tp_count, token_count, LANES), bf16),
+        pltpu.VMEM((token_count, ep_count * slot_rows), bf16),
+        pltpu.VMEM((token_count, ep_count * slot_rows), bf16),
+        pltpu.VMEM(out_weight.shape, bf16),
+        pltpu.VMEM(shared_down.shape, bf16),
         pltpu.VMEM((rows, lanes), bf16),
         pltpu.VMEM((rows, lanes), bf16),
         pltpu.VMEM((ep_count, pairs, 2, rows, LANES), bf16),
@@ -750,7 +915,7 @@
         pltpu.VMEM((tile, rows), f32),
         pltpu.VMEM((tile, LANES), f32),
         pltpu.VMEM((tile, LANES), f32),
-        pltpu.VMEM(ranks.shape, bf16),
+        pltpu.VMEM((ep_count, experts, token_count), f32),
     ]
     if not inside:
         scratch.append(pltpu.VMEM((token_count, depth), bf16))
@@ -759,9 +924,10 @@
         pltpu.VMEM((experts, depth, 2 * LANES), bf16),
         pltpu.VMEM(expert_down.shape, bf16),
         pltpu.VMEM((depth, 2 * LANES), bf16),
-        pltpu.VMEM((tp_count, ep_count, slot_rows, LANES), bf16),
+        pltpu.VMEM((tp_count, experts, ep_count * max(main, 1), LANES), bf16),
+        pltpu.VMEM((tp_count, max(ep_count * (slot_rows - experts * main), 8), LANES), bf16),
         pltpu.VMEM((ep_count, slot_rows, columns), bf16),
-        dma((6 + 2 * pairs,)),
+        dma((9 + 2 * pairs,)),
         dma((ep_count, pairs)),
         dma((ep_count, pairs)),
         dma((ep_count, pairs)),
@@ -770,14 +936,15 @@
         dma((chips,)),
         dma((ep_count, tp_count)),
         dma((ep_count, tp_count)),
+        dma((ep_count, 2)),
         dma((ep_count,)),
         dma((ep_count,)),
         dma((ep_count,)),
         dma((ep_count,)),
         dma((tp_count,)),
         dma((tp_count,)),
-        dma((tp_count,)),
-        dma((tp_count,)),
+        dma((experts + 1, tp_count)),
+        dma((experts + 1, tp_count)),
         dma((pairs, tp_count)),
         dma((pairs, tp_count)),
         dma((ep_count,)),
@@ -785,19 +952,19 @@
         dma((2,)),
     ]
     body = functools.partial(block_kernel, heads, main, tail)
-    inputs = 11
+    inputs = 15
 
     def kernel(*refs):
         refs = list(refs)
         if inside:
-            refs.insert(inputs + 3 + 17, None)
+            refs.insert(inputs + 2 + 27, None)
         body(*refs)
 
     blocks = ep_count * rows * rows * heads
-    results = pl.pallas_call(
+    return pl.pallas_call(
         kernel,
         out_shape=outs,
-        in_specs=[anywhere] * 3 + [vmem] * 3 + [anywhere] * 5,
+        in_specs=[anywhere] * 3 + [vmem] * 4 + [anywhere] * 8,
         out_specs=out_specs,
         scratch_shapes=scratch,
         compiler_params=pltpu.CompilerParams(
@@ -811,20 +978,19 @@
         query_rows,
         key_rows,
         value_rows,
-        cum_gate[:, None, :],
-        normed,
-        ranks,
+        cum_gate,
+        routes.T,
+        route_weight.T,
+        moe_gain[None, :],
+        moe_input,
         expert_gate,
         expert_up,
         expert_down,
         shared_gate,
         shared_up,
-    )
-    heads_all, returned, shared_all = results[:3]
-    if heads_all.ndim == 3:
-        heads_all = heads_all[:, :, :width].transpose(1, 0, 2).reshape(rows, -1)
-    shared_all = shared_all[:, :, :span].transpose(1, 0, 2).reshape(token_count, -1)
-    return heads_all, returned, shared_all
+        shared_down,
+        out_weight,
+    )[:2]
 
 
 def local(
@@ -844,64 +1010,24 @@
     shared_up,
     shared_down,
 ):
-    token_count = moe_input.shape[0]
-    top_count = routes.shape[1]
-    local_experts = expert_gate.shape[0]
-    ep_count = lax.axis_size("ep")
-    expert_count = local_experts * ep_count
-    capacity = 2 * token_count * top_count // expert_count
-    moe_rows = moe_input.astype(jnp.float32)
-    normed = (
-        moe_rows
-        * lax.rsqrt(jnp.mean(moe_rows * moe_rows, axis=1, keepdims=True) + norm_eps)
-        * moe_gain
-    ).astype(jnp.bfloat16)
-    expert_ids = jnp.arange(expert_count, dtype=jnp.int32)
-    chosen = routes[:, :, None] == expert_ids[None, None, :]
-    named = jnp.any(chosen, axis=1)
-    order = jnp.arange(token_count)
-    earlier = (order[None, :] < order[:, None]).astype(jnp.bfloat16)
-    ranks = jnp.dot(earlier, named.astype(jnp.bfloat16), preferred_element_type=jnp.float32)
-    ranks = jnp.where(named, ranks.astype(jnp.int32), -1)
-    rank_rows = ranks.astype(jnp.bfloat16).T.reshape(ep_count, local_experts, token_count)
-    heads_all, returned, shared_all = fused_block(
+    mixer, moe = fused_block(
         query_rows,
         key_rows,
         value_rows,
         cum_gate,
-        normed,
-        rank_rows,
-        capacity,
+        routes,
+        route_weight,
+        moe_gain,
+        moe_input,
         expert_gate,
         expert_up,
         expert_down,
         shared_gate,
         shared_up,
+        shared_down,
+        out_weight,
     )
-    main, tail, slot_rows = slot_layout(capacity, local_experts)
-    taken = jnp.sum(jnp.where(chosen, ranks[:, None, :], 0), axis=2)
-    local_id = routes % local_experts
-    spot = jnp.where(
-        taken < main,
-        local_id * main + taken,
-        local_experts * main + local_id * tail + taken - main,
-    )
-    spot = spot + routes // local_experts * slot_rows
-    spots = jnp.arange(ep_count * slot_rows, dtype=jnp.int32)
-    weight = jnp.zeros((token_count, ep_count * slot_rows), jnp.float32)
-    for choice in range(top_count):
-        hit = spot[:, choice : choice + 1] == spots[None, :]
-        weight = jnp.where(hit, route_weight[:, choice : choice + 1], weight)
-    weight_high = lax.reduce_precision(weight, 8, 7)
-    weight_low = weight - weight_high
-    results = returned.reshape(ep_count * slot_rows, -1)
-    moe_total = jnp.dot(shared_all, shared_down, preferred_element_type=jnp.float32)
-    for part in (weight_high, weight_low):
-        moe_total = moe_total + jnp.dot(
-            part.astype(jnp.bfloat16), results, preferred_element_type=jnp.float32
-        )
-    mixer_sum = jnp.dot(heads_all, out_weight, preferred_element_type=jnp.float32)
-    return (mixer_sum.astype(jnp.bfloat16), moe_total.astype(jnp.bfloat16))
+    return (mixer, moe)
 
 
 def solution(mesh):

time: 133 us -> 106 us (0.80)
  Pallas kernels: 118 us -> 101 us
  matrix products: 5.72 us -> 0 us
  other arithmetic: 5.48 us -> 0 us
    pallas_call x1, Pallas kernels: 118 us -> 101 us  [fused_block(): pl.pallas_call(kernel, out_shape=outs, in_specs=[anywhere] * 3 + [vmem] *...]
    dot_general x5 -> x0, matrix products: 5.72 us -> none  [the longest x1 3.4 us: local(): jnp.dot(heads_all, out_weight, preferred_element_type=jnp.float32)]
    unnamed x10 -> x2, local copies, waits for them, and re-layouts: 0.03 us -> 3.68 us
    reduce_sum x2 -> x0, other arithmetic: 2.24 us -> none  [the longest x1 1.5 us: local(): jnp.mean(moe_rows * moe_rows, axis=1, keepdims=True) + norm_eps]
    convert_element_type x2 -> x0, other arithmetic: 1.83 us -> none  [the longest x1 1.82 us: local(): normed = (moe_rows * lax.rsqrt(jnp.mean(moe_rows * moe_rows, axis=1, keep...]
    broadcast_in_dim x1 -> x0, local copies, waits for them, and re-layouts: 1.6 us -> none  [fused_block(): cum_gate[:, None, :]]
where the time goes in v3:
time: 106 us
  Pallas kernels  101 us (95%)
  local copies, waits for them, and re-layouts  3.68 us (3%)
    pallas_call x1, Pallas kernels, fused_block(): pl.pallas_call(kernel, out_shape=outs, in_specs=[anywhere] * 3 + [vmem] *...  101 us
    unnamed x2, local copies, waits for them, and re-layouts  3.68 us

profile of v3, /device:TPU:25, one launch (start us, length us, event | category | flops | bytes accessed | tf_op | source)
XLA Modules:
  0.0 105.7 jit_solution(1118201692568732391)
XLA Ops:
  0.6 101.4 %fused_block.1 = (bf16[768,512]{1,0:T(8,128)(2,1)}, bf16[192,512]{1,0:T(8,128)(2,1)}) custom-call(bf16[768,256]{1,0:T(8,128)(2,1)} %refs_0_.1, bf16[768,256]{1,0:T(8,128)(2,1)} %refs_1_.1, bf16[768,256]{1,0:T(8,128)(2,1)} %refs_2_.1, f32[4,6144]{1,0:T(4,128)} %refs_3_.1, s32[3,192]{1,0:T(4,128)} %bitcast.4, f32[3,192]{1,0:T(4,128)} %bitcast.5, ...), custom_call_target="tpu_custom_call" | custom-call | flops 19327352832 | bytes 8388608 | tf_op jit(solution)/shard_map/fused_block/pallas_call | solution.py:964
  102.1 2.1 %copy.19 = bf16[768,512]{1,0:T(8,128)(2,1)} copy(bf16[768,512]{1,0:T(8,128)(2,1)} %get-tuple-element.4) | data formatting | bytes 1572864
  104.1 1.6 %copy.20 = bf16[192,512]{1,0:T(8,128)(2,1)} copy(bf16[192,512]{1,0:T(8,128)(2,1)} %get-tuple-element.5) | data formatting | bytes 393216

commit v4 on v3

--- a/solution.py
+++ b/solution.py
@@ -118,7 +118,9 @@
     tp_me = lax.axis_index("tp")
     columns = normed_ref.shape[1] // tp_count
     last = chips - 1
-    host = chips - 2
+    host = chips - 3
+    limit = chips - 2
+    hops = 2 * CORES
     guests = chips > 2
 
     barrier = pltpu.get_barrier_semaphore()
@@ -280,7 +282,7 @@
             q_guest.at[:, lanes],
             guest_send.at[0, pair],
             guest_recv.at[0, pair],
-            ep=me - CORES,
+            ep=me - hops,
         )
 
     def guest_result(pair):
@@ -289,7 +291,7 @@
             guest_in.at[pair],
             guest_send.at[1, pair],
             guest_recv.at[1, pair],
-            ep=me + CORES,
+            ep=me + hops,
         )
 
     def guest_stats(pair):
@@ -298,17 +300,21 @@
             lse_in.at[pair],
             guest_send.at[2, pair],
             guest_recv.at[2, pair],
-            ep=me + CORES,
-        )
-
-    def chip_copy(target):
-        return remote(
-            normed_ref.at[:, lanes_at(tp_me, columns)],
-            tokens.at[me, :, lanes_at(tp_me, columns)],
-            chip_send.at[target],
-            piece_recv.at[me, tp_me],
-            ep=target * CORES + core,
-        )
+            ep=me + hops,
+        )
+
+    def hop_copy(slot, way, source=None):
+        place = tokens.at[slot, :, lanes_at(tp_me, columns)]
+        return remote(
+            place if source is None else source,
+            place,
+            chip_send.at[slot, way],
+            piece_recv.at[slot, tp_me],
+            ep=me + (CORES, -CORES)[way],
+        )
+
+    def own_hop(way):
+        return hop_copy(me, way, normed_ref.at[:, lanes_at(tp_me, columns)])
 
     def plane_copy(slot, piece, target):
         place = tokens.at[slot, :, lanes_at(piece, columns)]
@@ -386,19 +392,23 @@
         )
 
     loop(ep_count - 1, lambda turn: rank_copy(ep_at(turn), me).start())
-    loop(chips - 1, lambda turn: chip_copy(chip_at(turn)).start())
+    higher, lower = chip < last, chip > 0
+    pl.when(higher)(lambda: own_hop(0).start())
+    pl.when(lower)(lambda: own_hop(1).start())
     block_copy(normed_ref, me).start()
     picks[me] = rank_ref[me]
     for one in loads[1:]:
         one.wait()
 
+    paired = jnp.logical_and(chip == host, guests)
+
     for pair in range(pairs):
 
         @pl.when(chip < last)
         def _():
             up_copy(me, pair).start()
 
-        @pl.when(core == 0)
+        @pl.when(jnp.logical_or(core == 0, paired))
         def _():
             side_copy(me, pair).start()
 
@@ -459,14 +469,19 @@
                 score_unit(units[turn + 1], (turn + 1) % 2)
             value_unit(unit, turn % 2)
 
-    def spread_pieces(turn):
-        slot = chip_at(turn) * CORES + core
-        plane_copy(slot, tp_me, tp_me).wait_recv()
+    def spread_pieces(slot, way, onward):
+        hop_copy(slot, way).wait_recv()
+        pl.when(onward)(lambda: hop_copy(slot, way).start())
         if relay:
-            for way in range(2):
-                near_copy(slot, tp_me, way).start()
+            for near in range(2):
+                near_copy(slot, tp_me, near).start()
         else:
-            loop(tp_count - 1, lambda way: plane_copy(slot, tp_me, tp_at(way)).start())
+            loop(tp_count - 1, lambda peer: plane_copy(slot, tp_me, tp_at(peer)).start())
+
+    def spread_distance(turn):
+        down_slot, up_slot = me - (turn + 1) * CORES, me + (turn + 1) * CORES
+        pl.when(down_slot >= 0)(lambda: spread_pieces(down_slot, 0, higher))
+        pl.when(up_slot < ep_count)(lambda: spread_pieces(up_slot, 1, lower))
 
     def relay_pieces(turn):
         slot = chip_at(turn) * CORES + core
@@ -475,7 +490,7 @@
             half_copy(slot, peer, way).start()
 
     def token_stage():
-        loop(chips - 1, spread_pieces)
+        loop(chips - 1, spread_distance)
         if relay:
             loop(chips - 1, relay_pieces)
 
@@ -653,7 +668,7 @@
     reach = 1 if guests else chips
     deepest = jnp.where(chip == last, jnp.minimum(chip, reach), chip)
     step_count = deepest * CORES + core
-    steps = max(CORES * (host if guests else last) + 1, CORES + 1)
+    steps = max(CORES * (limit if guests else last) + 1, CORES + 1)
     delay = 3 if guests else 1
     total = pairs * (steps + 1)
 
@@ -664,7 +679,7 @@
         slot = (chip - back) * CORES + jnp.where(own_core, core, other)
         side_copy(slot, pair).wait_recv()
 
-        @pl.when(jnp.logical_and(own_core, chip < (host if guests else last)))
+        @pl.when(jnp.logical_and(own_core, chip < (limit if guests else last)))
         def _():
             up_copy(slot, pair).start()
 
@@ -675,17 +690,22 @@
         attend(pair, slot, q_own, acc, row_max, False)
         if guests:
 
-            @pl.when(jnp.logical_and(chip == host, back >= 1))
+            @pl.when(chip == host)
             def _():
-                @pl.when(step == core)
-                def _():
-                    guest_query(pair).wait_recv()
-                    for member in range(group):
-                        head = pair * group + member
-                        guest_acc[head] = jnp.zeros((rows, LANES), jnp.float32)
-                        guest_max[head] = jnp.full((rows, LANES), neg_fill, jnp.float32)
-
                 attend(pair, slot, q_guest, guest_acc, guest_max, False)
+
+    def start_guest(pair):
+        guest_query(pair).wait_recv()
+        for member in range(group):
+            head = pair * group + member
+            guest_acc[head] = jnp.zeros((rows, LANES), jnp.float32)
+            guest_max[head] = jnp.full((rows, LANES), neg_fill, jnp.float32)
+
+        def own_chip(turn):
+            pl.when(turn > 0)(lambda: side_copy(me + 1, pair).wait_recv())
+            attend(pair, me + turn, q_guest, guest_acc, guest_max, False)
+
+        loop(CORES - core, own_chip)
 
     hooks = (
         (1, shared_stage),
@@ -709,6 +729,12 @@
             pair = (index - pairs) // steps
             step = (index - pairs) % steps
 
+            if guests:
+
+                @pl.when(jnp.logical_and(chip == host, step == 0))
+                def _():
+                    start_guest(pair)
+
             @pl.when(step < step_count)
             def _():
                 remote_step(pair, step)
@@ -736,7 +762,7 @@
 
             @pl.when(
                 jnp.logical_or(
-                    chip < (host if guests else last), jnp.logical_and(back == 0, chip < last)
+                    chip < (limit if guests else last), jnp.logical_and(back == 0, chip < last)
                 )
             )
             def _():
@@ -748,7 +774,7 @@
 
         loop(deepest + 1, finish_kv)
 
-        @pl.when(core == 0)
+        @pl.when(jnp.logical_or(core == 0, paired))
         def _():
             side_copy(me, pair).wait_send()
 
@@ -766,7 +792,8 @@
     def finish_tokens(turn):
         target = chip_at(turn)
         slot = target * CORES + core
-        chip_copy(target).wait_send()
+        pl.when(jnp.logical_and(target < chip, higher))(lambda: hop_copy(slot, 0).wait_send())
+        pl.when(jnp.logical_and(target > chip, lower))(lambda: hop_copy(slot, 1).wait_send())
         if relay:
             for way, peer in enumerate((x_peer, y_peer)):
                 near_copy(slot, tp_me, way).wait_send()
@@ -776,6 +803,8 @@
         block_copy(tokens.at[slot], slot).wait_send()
 
     loop(chips - 1, finish_tokens)
+    pl.when(higher)(lambda: own_hop(0).wait_send())
+    pl.when(lower)(lambda: own_hop(1).wait_send())
     block_copy(normed_ref, me).wait_send()
 
     def finish_peers(turn):
@@ -933,7 +962,7 @@
         dma((ep_count, pairs)),
         dma((3, pairs)),
         dma((3, pairs)),
-        dma((chips,)),
+        dma((ep_count, 2)),
         dma((ep_count, tp_count)),
         dma((ep_count, tp_count)),
         dma((ep_count, 2)),

time: 106 us -> 104 us (0.981)
  the two profiles are of different devices: /device:TPU:25 before, /device:TPU:9 now
where the time goes in v4:
time: 104 us
  Pallas kernels  99.5 us (96%)
  local copies, waits for them, and re-layouts  3.68 us (4%)
    pallas_call x1, Pallas kernels, fused_block(): pl.pallas_call(kernel, out_shape=outs, in_specs=[anywhere] * 3 + [vmem] *...  99.5 us
    unnamed x2, local copies, waits for them, and re-layouts  3.68 us

profile of v4, /device:TPU:9, one launch (start us, length us, event | category | flops | bytes accessed | tf_op | source)
XLA Modules:
  0.0 103.8 jit_solution(5911033444670325047)
XLA Ops:
  0.6 99.5 %fused_block.1 = (bf16[768,512]{1,0:T(8,128)(2,1)}, bf16[192,512]{1,0:T(8,128)(2,1)}) custom-call(bf16[768,256]{1,0:T(8,128)(2,1)} %refs_0_.1, bf16[768,256]{1,0:T(8,128)(2,1)} %refs_1_.1, bf16[768,256]{1,0:T(8,128)(2,1)} %refs_2_.1, f32[4,6144]{1,0:T(4,128)} %refs_3_.1, s32[3,192]{1,0:T(4,128)} %bitcast.4, f32[3,192]{1,0:T(4,128)} %bitcast.5, ...), custom_call_target="tpu_custom_call" | custom-call | flops 19327352832 | bytes 8388608 | tf_op jit(solution)/shard_map/fused_block/pallas_call | solution.py:993
  100.2 2.1 %copy.19 = bf16[768,512]{1,0:T(8,128)(2,1)} copy(bf16[768,512]{1,0:T(8,128)(2,1)} %get-tuple-element.4) | data formatting | bytes 1572864
  102.2 1.6 %copy.20 = bf16[192,512]{1,0:T(8,128)(2,1)} copy(bf16[192,512]{1,0:T(8,128)(2,1)} %get-tuple-element.5) | data formatting | bytes 393216
